TPU v7x, 32 devices: a whole 2x2x4 slice. The times are simulated.
32 devices in a mesh: grp: 2 (over y), sp: 4 (over z), tp: 4 (over x, core).
Axes of the slice: x: 2, y: 2, z: 4, core: 2. Of those that a mesh axis runs over, the one named last changes fastest.
Arguments:
- residual: bfloat16 [3072, 2048], P(('grp', 'sp', 'tp')), parts along dimension 0, may hold values from -36 to 36
- query: bfloat16 [3072, 512], P(('grp', 'sp'), 'tp'), parts along dimension 0, may hold values from -6 to 6
- keys: bfloat16 [3072, 512], P(('grp', 'sp'), 'tp'), parts along dimension 0, may hold values from -6 to 6
- values: bfloat16 [3072, 1024], P(('grp', 'sp'), 'tp'), parts along dimension 0, may hold values from -6 to 6
- out_gate: bfloat16 [3072, 1024], P(('grp', 'sp'), 'tp'), parts along dimension 0, may hold values from -6 to 6
- input_gate: float32 [2, 4, 3072], P(None, 'tp', ('grp', 'sp')), parts along dimension 2, may hold values from -5 to 95
- forget_gate: float32 [2, 4, 3072], P(None, 'tp', ('grp', 'sp')), parts along dimension 2, may hold values from -6 to 20
- head_gain: float32 [1024], P('tp'), may hold values from 0.1 to 1.9
- w_out: bfloat16 [1024, 2048], P('tp'), may hold values from -0.1875 to 0.1875
- norm_gain: float32 [2048], replicated, may hold values from 0.1 to 1.9
- w_up_gate: bfloat16 [2048, 5632], P('sp', 'tp'), may hold values from -0.125 to 0.125
- w_up_value: bfloat16 [2048, 5632], P('sp', 'tp'), may hold values from -0.125 to 0.125
- conv_gate: float32 [3, 5632], P(None, 'tp'), may hold values from -3 to 3
- conv_value: float32 [3, 5632], P(None, 'tp'), may hold values from -3 to 3
- w_down: bfloat16 [5632, 2048], P('tp', 'sp'), may hold values from -0.078125 to 0.078125
Outputs:
- layer_out: bfloat16 [3072, 2048], P(('grp', 'sp', 'tp')), parts along dimension 0
There are 2 independent parts, one for each index of `grp`. A program takes and returns all parts, laid end to end along the dimension named above; an argument that names none is the same for every part. Nothing has to cross between parts.
All inputs are finite; a program needn't handle non-finite values.
Results may differ from a plain program's by a relative error of at most 0.011.
Values may be sent and summed in bfloat16 or wider, within the bound.
No kernel may reach another device: no remote copies, remote signals or barrier semaphores. Data moves between devices by JAX's collectives and lax.ppermute only.
A program may use at most 128 MiB of HBM per device.

v0:
```python
import jax
import jax.numpy as jnp
from jax import lax
from jax.sharding import PartitionSpec as P

QK_DIM = 128
V_DIM = 256
CONV = 3


epsilon = 1e-06
floor_log = -1e30
highest = lax.Precision.HIGHEST


def entering(value, axis, join, neutral, backward):
    count, mine = (lax.axis_size(axis), lax.axis_index(axis))
    pieces = jax.tree.map(lambda part: lax.all_gather(part, axis), value)
    if backward:
        pieces = jax.tree.map(lambda part: part[::-1], pieces)
        mine = count - 1 - mine
    total = jax.tree.map(
        lambda part, zero: jnp.full_like(part, 0) + jnp.asarray(zero, part.dtype), value, neutral
    )

    def step(position, total):
        longer = join(total, jax.tree.map(lambda part: part[position], pieces))
        return jax.tree.map(lambda new, old: jnp.where(position < mine, new, old), longer, total)

    return lax.fori_loop(0, count - 1, step, total)


def extended(x, sides, width):
    for axis, dim in sides:
        size, length = (lax.axis_size(axis), x.shape[dim])
        up = [(i, (i + 1) % size) for i in range(size - 1)]
        down = [(j, i) for i, j in up]
        last = lax.slice_in_dim(x, length - width, length, axis=dim)
        initial = lax.slice_in_dim(x, 0, width, axis=dim)
        before = lax.ppermute(last, axis, up)
        after = lax.ppermute(initial, axis, down)
        x = jnp.concatenate([before, x, after], axis=dim)
    return x


def summarize(keys_scaled, values_wide, in_gate, log_cum):
    totals = log_cum[:, -1]
    growth = totals[:, None] - log_cum + in_gate
    largest = jnp.max(growth, axis=-1)
    weighting = jnp.exp(growth - largest[:, None])
    weighted = keys_scaled * jnp.transpose(weighting)[:, :, None]
    memory = jnp.einsum("shd,she->hde", weighted, values_wide, precision=highest)
    return (totals, memory, jnp.sum(weighted, axis=0), largest)


def combine(early, later):
    early_total, early_memory, early_normalizer, early_top = early
    later_total, later_memory, later_normalizer, later_top = later
    carried = early_top + later_total
    joint_top = jnp.maximum(carried, later_top)
    early_scale = jnp.exp(carried - joint_top)
    later_scale = jnp.exp(later_top - joint_top)
    memory = early_scale[:, None, None] * early_memory + later_scale[:, None, None] * later_memory
    normalizer = early_scale[:, None] * early_normalizer + later_scale[:, None] * later_normalizer
    return (early_total + later_total, memory, normalizer, joint_top)


def prepare(keys_heads, value_heads, in_gate, forget_pre):
    log_cum = jnp.cumsum(jax.nn.log_sigmoid(forget_pre), axis=-1)
    keys_scaled = keys_heads.astype(jnp.float32) * QK_DIM ** (-0.5)
    return (log_cum, summarize(keys_scaled, value_heads.astype(jnp.float32), in_gate, log_cum))


def read_out(query_heads, keys_heads, value_heads, in_gate, log_cum, state):
    memory, normalizer, top_in = (state[1], state[2], state[3])
    length = query_heads.shape[0]
    lower_tri = jnp.tril(jnp.ones((length, length), dtype=bool))
    exponent = jnp.where(
        lower_tri[None], log_cum[:, :, None] - log_cum[:, None, :] + in_gate[:, None, :], -jnp.inf
    )
    before = log_cum + top_in[:, None]
    running = jnp.maximum(before, jnp.max(exponent, axis=-1))
    carry_scale = jnp.exp(before - running)
    scores = jnp.einsum(
        "thd,shd->hts", query_heads, keys_heads, preferred_element_type=jnp.float32
    ) * QK_DIM ** (-0.5)
    weights = jnp.exp(exponent - running[:, :, None]) * scores
    query_wide = query_heads.astype(jnp.float32)
    numerator = carry_scale[:, :, None] * jnp.einsum(
        "thd,hde->hte", query_wide, memory, precision=highest
    )
    numerator = numerator + jnp.einsum(
        "hts,she->hte",
        weights.astype(jnp.bfloat16),
        value_heads,
        preferred_element_type=jnp.float32,
    )
    denominator = carry_scale * jnp.einsum(
        "thd,hd->ht", query_wide, normalizer, precision=highest
    ) + jnp.sum(weights, axis=-1)
    return numerator / jnp.maximum(jnp.abs(denominator), jnp.exp(-running))[:, :, None]


def local(
    residual,
    query,
    keys,
    values,
    out_gate,
    input_gate,
    forget_gate,
    head_gain,
    w_out,
    norm_gain,
    w_up_gate,
    w_up_value,
    conv_gate,
    conv_value,
    w_down,
):
    length = query.shape[0]
    heads_here = input_gate.shape[1]
    query_heads = query.reshape(length, heads_here, QK_DIM)
    keys_heads = keys.reshape(length, heads_here, QK_DIM)
    value_heads = values.reshape(length, heads_here, V_DIM)
    query_back = query_heads[::-1]
    keys_back = keys_heads[::-1]
    value_back = value_heads[::-1]
    back_gate = input_gate[1][:, ::-1]
    ahead_cum, ahead_summary = prepare(keys_heads, value_heads, input_gate[0], forget_gate[0])
    behind_cum, behind_summary = prepare(keys_back, value_back, back_gate, forget_gate[1][:, ::-1])
    identity = (
        jnp.zeros((heads_here,), jnp.float32),
        jnp.zeros((heads_here, QK_DIM, V_DIM), jnp.float32),
        jnp.zeros((heads_here, QK_DIM), jnp.float32),
        jnp.full((heads_here,), floor_log, jnp.float32),
    )
    ahead_state = entering(ahead_summary, "sp", combine, identity, False)
    behind_state = entering(behind_summary, "sp", combine, identity, True)
    ahead = read_out(query_heads, keys_heads, value_heads, input_gate[0], ahead_cum, ahead_state)
    behind = read_out(query_back, keys_back, value_back, back_gate, behind_cum, behind_state)[
        :, ::-1
    ]
    both = ahead + behind
    scaled = both * lax.rsqrt(jnp.mean(both * both, axis=-1, keepdims=True) + epsilon)
    scaled = scaled * head_gain.reshape(heads_here, V_DIM)[:, None, :]
    side_by_side = jnp.transpose(scaled, (1, 0, 2)).reshape(length, heads_here * V_DIM)
    gated = (side_by_side * jax.nn.sigmoid(out_gate.astype(jnp.float32))).astype(jnp.bfloat16)
    row_heads = lax.all_to_all(gated, "tp", split_axis=0, concat_axis=1, tiled=True)
    columns = row_heads
    projected = jnp.dot(
        columns, lax.all_gather(w_out, "tp", axis=0, tiled=True), preferred_element_type=jnp.float32
    )
    stream = (residual.astype(jnp.float32) + projected).astype(jnp.bfloat16)
    stream_wide = stream.astype(jnp.float32)
    normed = stream_wide * lax.rsqrt(
        jnp.mean(stream_wide * stream_wide, axis=-1, keepdims=True) + epsilon
    )
    normed = (normed * norm_gain).astype(jnp.bfloat16)
    whole = lax.all_gather(normed, "tp", axis=0, tiled=True)
    width_ff = w_up_gate.shape[1]
    columns = whole
    up_gate = jnp.dot(
        columns,
        lax.all_gather(w_up_gate, "sp", axis=0, tiled=True),
        preferred_element_type=jnp.float32,
    )
    up_value = jnp.dot(
        columns,
        lax.all_gather(w_up_value, "sp", axis=0, tiled=True),
        preferred_element_type=jnp.float32,
    )
    upper = jnp.concatenate([up_gate, up_value], axis=1).astype(jnp.bfloat16)
    padded = extended(upper, (("sp", 0),), CONV // 2)
    taps = jnp.concatenate([conv_gate, conv_value], axis=1)
    smeared = padded[0:length] * taps[0]
    for offset in range(1, CONV):
        smeared = smeared + padded[offset : offset + length] * taps[offset]
    hidden = (jax.nn.silu(smeared[:, :width_ff]) * smeared[:, width_ff:]).astype(jnp.bfloat16)
    terms = jnp.dot(
        hidden, lax.all_gather(w_down, "sp", axis=1, tiled=True), preferred_element_type=jnp.float32
    )
    returned = lax.psum_scatter(
        terms.astype(jnp.bfloat16), "tp", scatter_dimension=0, tiled=True
    ).astype(jnp.float32)
    return (stream_wide + returned).astype(jnp.bfloat16)


def solution(mesh):
    placed = (
        P(("grp", "sp", "tp"), None),
        P(("grp", "sp"), "tp"),
        P(("grp", "sp"), "tp"),
        P(("grp", "sp"), "tp"),
        P(("grp", "sp"), "tp"),
        P(None, "tp", ("grp", "sp")),
        P(None, "tp", ("grp", "sp")),
        P("tp"),
        P("tp", None),
        P(),
        P("sp", "tp"),
        P("sp", "tp"),
        P(None, "tp"),
        P(None, "tp"),
        P("tp", "sp"),
    )
    return jax.shard_map(
        local, mesh=mesh, in_specs=placed, out_specs=P(("grp", "sp", "tp"), None), check_vma=False
    )
```

profile of v0, /device:TPU:0, one launch (start us, length us, event | category | flops | bytes accessed | tf_op | source)
XLA Modules:
  0.0 504.6 jit_solution(14796732401205961232)
XLA Ops:
  6.5 0.7 all-gather.12.cloned.1.call-update
  7.3 0.7 negate_reduce_fusion
  9.1 0.6 slice.80
  9.7 0.7 slice_reduce_fusion.5
  11.5 0.6 slice.79
  12.1 2.0 fusion.44
  14.1 1.2 dynamic-slice
  15.3 1.2 bitcast_dynamic-update-slice_fusion.1
  16.6 1.3 bitcast_dynamic-update-slice_fusion
  17.9 1.2 fusion.49
  19.2 1.2 multiply_reduce_fusion.2
  20.4 1.3 dynamic-update-slice.3
  21.7 1.4 dynamic-update-slice.1
  23.1 13.5 %all-reduce.4 = (f32[4]{0:T(128)S(1)}, f32[4]{0:T(128)S(1)}, f32[4]{0:T(128)S(1)}, f32[4]{0:T(128)S(1)}) all-reduce(f32[4]{0:T(128)S(1)} %bitcast_dynamic-update-slice_fusion, f32[4]{0:T(128)S(1)} %dynamic-update-slice.3, f32[4]{0:T(128)S(1)} %bitcast_dynamic-update-slice_fusion.1, ...), channel_id=1, replica_groups=mesh['grp'=2,'sp'=4,'tp'=4] {'sp'}, use_global_device_ids=true, to_apply=%add.2 | all-reduce | flops 16 | bytes 128
  36.8 1.6 reverse.12
  38.4 2.4 reverse.13
  41.4 14.8 %all-gather.2 = f32[512,256]{1,0:T(8,128)S(1)} all-gather(f32[128,256]{1,0:T(8,128)S(1)} %fusion.29), channel_id=4, replica_groups=mesh['grp'=2,'sp'=4,'tp'=4] {'sp'}, dimensions={0}, use_global_device_ids=true | all-gather | bytes 655360 | tf_op jit(solution)/shard_map/all_gather | solution.py:18
  56.2 8.1 %all-gather.5 = f32[4,1,128]{2,1,0:T(1,128)S(1)} all-gather(f32[1,1,128]{2,1,0:T(1,128)S(1)} %bitcast.205), channel_id=5, replica_groups=mesh['grp'=2,'sp'=4,'tp'=4] {'sp'}, dimensions={0}, use_global_device_ids=true | all-gather | bytes 2560 | tf_op jit(solution)/shard_map/all_gather | solution.py:18
  64.3 8.4 %while.37 = (s32[]{:T(128)}, f32[1,128,256]{2,1,0:T(8,128)S(1)}, f32[1,128]{1,0:T(1,128)S(1)}, f32[1]{0:T(128)}, s32[]{:T(128)}, /*index=5*/f32[4,1]{0,1:T(1,128...) while((s32[]{:T(128)}, f32[1,128,256]{2,1,0:T(8,128)S(1)}, ...), condition=%wide.region_13.14_spmd.clone, body=%wide.region_12.13_spmd.clone.sunk | while | flops 164489 | bytes 395004 | solution.py:30
  64.3 0.6 constant_dynamic-slice_fusion.9
  67.1 0.7 constant_dynamic-slice_fusion.9
  69.9 0.7 constant_dynamic-slice_fusion.9
  74.5 0.5 reverse.15
  75.2 1.4 exponential_multiply_fusion
  76.7 9.0 %all-gather.4 = f32[4,1,128]{2,1,0:T(1,128)S(1)} all-gather(f32[1,1,128]{2,1,0:T(1,128)S(1)} %bitcast.206), channel_id=3, replica_groups=mesh['grp'=2,'sp'=4,'tp'=4] {'sp'}, dimensions={0}, use_global_device_ids=true | all-gather | bytes 2560 | tf_op jit(solution)/shard_map/all_gather | solution.py:18
  86.2 14.7 %all-gather = f32[512,256]{1,0:T(8,128)S(1)} all-gather(f32[128,256]{1,0:T(8,128)S(1)} %fusion.31), channel_id=2, replica_groups=mesh['grp'=2,'sp'=4,'tp'=4] {'sp'}, dimensions={0}, use_global_device_ids=true | all-gather | bytes 655360 | tf_op jit(solution)/shard_map/all_gather | solution.py:18
  100.9 8.3 %while.36 = (s32[]{:T(128)}, f32[1,128,256]{2,1,0:T(8,128)S(1)}, f32[1,128]{1,0:T(1,128)S(1)}, f32[1]{0:T(128)}, s32[]{:T(128)}, /*index=5*/f32[4,1]{0,1:T(1,128...) while((s32[]{:T(128)}, f32[1,128,256]{2,1,0:T(8,128)S(1)}, ...), condition=%wide.region_5.6_spmd.clone, body=%wide.region_4.5_spmd.clone.sunk | while | flops 164489 | bytes 395004 | solution.py:30
  100.9 0.7 constant_dynamic-slice_fusion.8
  103.7 0.7 constant_dynamic-slice_fusion.8
  106.5 0.7 constant_dynamic-slice_fusion.8
  111.1 7.9 %all_to_all.19 = bf16[4,96,256]{2,1,0:T(8,128)(2,1)S(1)} all-to-all(bf16[4,96,256]{2,1,0:T(8,128)(2,1)S(1)} %bitcast.196), channel_id=1, replica_groups=mesh['grp'=2,'sp'=4,'tp'=4] {'tp'}, dimensions={0} | all-to-all | bytes 393216 | tf_op jit(solution)/shard_map/all_to_all | solution.py:149
  119.0 3.1 multiply_reduce_fusion
  122.2 0.9 multiply_convert_fusion
  123.2 0.7 all-gather.18.cloned.1.call-update
  124.5 0.5 all-gather.20.cloned.1.call-update
  125.1 15.4 %all-gather.14.cloned.1.call-done = bf16[384,2048]{1,0:T(8,128)(2,1)} async-done(((bf16[96,2048]{1,0:T(8,128)(2,1)}), bf16[384,2048]{1,0:T(8,128)(2,1)}) %all-gather.14.cloned.1.call-update) | async-done | bytes 1572880 | tf_op jit(solution)/shard_map/all_gather | solution.py:160
  140.5 108.3 %all-gather.18.cloned.1.call-done = bf16[2048,1408]{1,0:T(8,128)(2,1)} async-done(((bf16[512,1408]{1,0:T(8,128)(2,1)}), bf16[2048,1408]{1,0:T(8,128)(2,1)}) %all-gather.18.cloned.1.call-update) | async-done | bytes 5767184 | tf_op jit(solution)/shard_map/all_gather | solution.py:170
  248.8 5.7 %convolution_convert_fusion.1 = bf16[384,1408]{1,0:T(8,128)(2,1)S(1)} fusion(bf16[384,2048]{1,0:T(8,128)(2,1)} %all-gather.14.cloned.1.call-done, bf16[2048,1408]{1,0:T(8,128)(2,1)} %all-gather.18.cloned.1.call-done), kind=kOutput, calls=%fused_computation.22 | convolution fusion | flops 2215133184 | bytes 8421376 | tf_op jit(solution)/shard_map/dot_general | solution.py:168
  254.5 100.7 %all-gather.16.cloned.1.call-done = bf16[2048,1408]{1,0:T(8,128)(2,1)} async-done(((bf16[512,1408]{1,0:T(8,128)(2,1)}), bf16[2048,1408]{1,0:T(8,128)(2,1)}) %all-gather.16.cloned.1.call-update) | async-done | bytes 5767184 | tf_op jit(solution)/shard_map/all_gather | solution.py:165
  355.2 5.2 %convolution_convert_fusion.2 = bf16[384,1408]{1,0:T(8,128)(2,1)S(1)} fusion(bf16[384,2048]{1,0:T(8,128)(2,1)S(1)} %copy-done.9, bf16[2048,1408]{1,0:T(8,128)(2,1)} %all-gather.16.cloned.1.call-done), kind=kOutput, calls=%fused_computation.23 | convolution fusion | flops 2215133184 | bytes 8421376 | tf_op jit(solution)/shard_map/dot_general | solution.py:163
  360.5 1.3 collective-permute-start
  361.8 1.5 collective-permute-start.1
  363.4 4.1 collective-permute-done.1
  367.5 4.3 multiply_add_fusion
  371.8 90.0 %all-gather.20.cloned.1.call-done = bf16[1408,2048]{1,0:T(8,128)(2,1)} async-done(((bf16[1408,512]{1,0:T(8,128)(2,1)}), bf16[1408,2048]{1,0:T(8,128)(2,1)}) %all-gather.20.cloned.1.call-update) | async-done | bytes 5767184 | tf_op jit(solution)/shard_map/all_gather | solution.py:181
  461.7 7.7 %convolution_convert_fusion = bf16[384,2048]{1,0:T(8,128)(2,1)} fusion(bf16[1408,2048]{1,0:T(8,128)(2,1)} %all-gather.20.cloned.1.call-done, f32[384,2816]{1,0:T(8,128)} %multiply_add_fusion), kind=kOutput, calls=%fused_computation.21 | convolution fusion | flops 2218622976 | bytes 11665408 | tf_op jit(solution)/shard_map/dot_general | solution.py:180
  469.5 26.4 %reduce-scatter.2.cloned.1.call-done = bf16[96,2048]{1,0:T(8,128)(2,1)} async-done(((bf16[384,2048]{1,0:T(8,128)(2,1)}), bf16[96,2048]{1,0:T(8,128)(2,1)}) %reduce-scatter.2.cloned.1.call-update) | async-done | bytes 393232 | tf_op jit(solution)/shard_map/reduce_scatter | solution.py:183
  495.9 1.8 add_convert_fusion
  (101 shorter events, 8.6 us)
Async XLA Ops:
  6.5 112.5 %all-gather.12.cloned.1.call-start = ((), (), s32[]{:S(2)}) async-start(), calls=%async_computation.2 | async-start | bytes 5242880 | tf_op jit(solution)/shard_map/all_gather | solution.py:152
  7.3 133.3 %all-gather.14.cloned.1.call-start = ((), (), s32[]{:S(2)}) async-start(), calls=%async_computation.3 | async-start | bytes 1966080 | tf_op jit(solution)/shard_map/all_gather | solution.py:160
  40.9 31.8 %copy-start.3 = (bf16[384,128]{1,0:T(8,128)(2,1)S(1)}, bf16[384,128]{1,0:T(8,128)(2,1)}, u32[]{:S(2)}) copy-start(bf16[384,128]{1,0:T(8,128)(2,1)} %param.20) | copy-start | bytes 294916
  73.4 1.7 copy-start.4
  73.7 2.9 copy-start.1
  73.7 12.1 %copy-start = (bf16[384,256]{1,0:T(8,128)(2,1)S(1)}, bf16[384,256]{1,0:T(8,128)(2,1)}, u32[]{:S(2)}) copy-start(bf16[384,256]{1,0:T(8,128)(2,1)} %param.22) | copy-start | bytes 589828
  109.6 1.2 copy-start.8
  110.0 9.0 %copy-start.2 = (bf16[96,2048]{1,0:T(8,128)(2,1)S(1)}, bf16[96,2048]{1,0:T(8,128)(2,1)}, u32[]{:S(2)}) copy-start(bf16[96,2048]{1,0:T(8,128)(2,1)} %param.19) | copy-start | bytes 1179652
  119.0 3.2 copy-start.7
  123.1 2.0 copy-start.5
  123.1 2.0 copy-start.6
  123.1 125.7 %all-gather.18.cloned.1.call-start = ((), (), s32[]{:S(2)}) async-start(), calls=%async_computation.5 | async-start | bytes 7208960 | tf_op jit(solution)/shard_map/all_gather | solution.py:170
  123.9 231.4 %all-gather.16.cloned.1.call-start = ((), (), s32[]{:S(2)}) async-start(), calls=%async_computation.4 | async-start | bytes 7208960 | tf_op jit(solution)/shard_map/all_gather | solution.py:165
  124.4 337.3 %all-gather.20.cloned.1.call-start = ((), (), s32[]{:S(2)}) async-start(), calls=%async_computation.6 | async-start | bytes 7208960 | tf_op jit(solution)/shard_map/all_gather | solution.py:181
  125.0 370.9 %reduce-scatter.2.cloned.1.call-start = ((), (), s32[]{:S(2)}) async-start(), calls=%async_computation.7 | async-start | bytes 1966080 | tf_op jit(solution)/shard_map/reduce_scatter | solution.py:183
  140.5 214.7 %copy-start.9 = (bf16[384,2048]{1,0:T(8,128)(2,1)S(1)}, bf16[384,2048]{1,0:T(8,128)(2,1)}, u32[]{:S(2)}) copy-start(bf16[384,2048]{1,0:T(8,128)(2,1)} %all-gather.14.cloned.1.call-done) | copy-start | bytes 4718596
  360.5 2.9 collective-permute-start
  361.8 5.7 %collective-permute-start.1 = (bf16[1,2816]{1,0:T(2,128)(2,1)S(1)}, bf16[1,2816]{1,0:T(2,128)(2,1)S(1)}, u32[]{:S(2)}, u32[]{:S(2)}) collective-permute-start(bf16[1,2816]{1,0:T(2,128)(2,1)S(1)} %get-tuple-element.466), channel_id=1, source_target_pairs={{4,0},{8,4},{12,8},{5,1},{9,5},{13,9},{6,2},{10,6},{14,10},{7,3},{... | collective-permute-start | bytes 16904 | tf_op jit(solution)/shard_map/ppermute | solution.py:41
Sparse Core Ops, SparseCore 0:
  8.9 37.1 all-gather.11
  123.2 17.2 all-gather.13
  142.1 106.6 all-gather.17
  250.2 104.9 all-gather.15
  356.6 105.0 all-gather.19
  469.6 26.2 reduce-scatter.1
where the time goes:
time: 506 us; the launch traced here: 505 us
  waiting for transfers between devices  347 us (69%)
  blocking collectives  67.9 us (13%)
  matrix products  25.3 us (5%)
  local copies, waits for them, and re-layouts  18.8 us (4%)
  other arithmetic  16.1 us (3%)
  between operations  13.9 us (3%)
  loops' own time  12.3 us (2%)
    all_gather x1, waiting for transfers between devices, local(): lax.all_gather(w_up_value, 'sp', axis=0, tiled=True)  108 us
    all_gather x1, waiting for transfers between devices, local(): lax.all_gather(w_up_gate, 'sp', axis=0, tiled=True)  101 us
    all_gather x1, waiting for transfers between devices, local(): lax.all_gather(w_down, 'sp', axis=1, tiled=True)  90 us
    all_gather x4, blocking collectives, entering(): pieces = jax.tree.map(lambda part: lax.all_gather(part, axis), value)  46.6 us
    reduce_scatter x1, waiting for transfers between devices, local(): lax.psum_scatter(terms.astype(jnp.bfloat16), 'tp', scatter_dimension=0, t...  26.4 us
    all_gather x1, waiting for transfers between devices, local(): whole = lax.all_gather(normed, 'tp', axis=0, tiled=True)  15.4 us
    unnamed x1, blocking collectives  13.5 us
    another operation x2, loops' own time, entering(): return lax.fori_loop(0, count - 1, step, total)  12.3 us
  transfers between devices with their start and end apart: 8, of which 6 were waited for; matrix products, arithmetic and copies ran while one was open for 9% of the time, Pallas kernels for 0%

commit v1 on v0

v1 whole, which is shorter than its diff:
```python
import jax
import jax.numpy as jnp
from jax import lax
from jax.sharding import PartitionSpec as P

QK_DIM = 128
V_DIM = 256
CONV = 3


epsilon = 1e-06
floor_log = -1e30
highest = lax.Precision.HIGHEST


def swap(x, axis, distance):
    size = lax.axis_size(axis)
    return lax.ppermute(x, axis, [(i, i ^ distance) for i in range(size)])


def shifted(x, axis, distance):
    size = lax.axis_size(axis)
    pairs = [(i, i + distance) for i in range(size) if 0 <= i + distance < size]
    return lax.ppermute(x, axis, pairs)


def pick(x, index, dim):
    return lax.dynamic_index_in_dim(x, index, axis=dim, keepdims=False)


def in_order(mine, other, bit, dim):
    first = jnp.where(bit == 0, mine, other)
    second = jnp.where(bit == 0, other, mine)
    return jnp.stack([first, second], axis=dim)


def combine(early, later):
    early_total, early_memory, early_normalizer, early_top = early
    later_total, later_memory, later_normalizer, later_top = later
    carried = early_top + later_total
    joint_top = jnp.maximum(carried, later_top)
    early_scale = jnp.exp(carried - joint_top)
    later_scale = jnp.exp(later_top - joint_top)
    memory = early_scale[:, None, None] * early_memory + later_scale[:, None, None] * later_memory
    normalizer = early_scale[:, None] * early_normalizer + later_scale[:, None] * later_normalizer
    return (early_total + later_total, memory, normalizer, joint_top)


def pack(state):
    total, memory, normalizer, top = state
    heads, _, width = memory.shape
    row = jnp.pad(normalizer, ((0, 0), (0, width - normalizer.shape[1])))
    scalars = jnp.pad(jnp.stack([total, top], axis=1), ((0, 0), (0, width - 2)))
    extra = jnp.stack([row, scalars], axis=1)
    return jnp.concatenate([memory, jnp.pad(extra, ((0, 0), (0, 6), (0, 0)))], axis=1)


def unpack(packed, present):
    memory = packed[:, :QK_DIM]
    normalizer = packed[:, QK_DIM, :QK_DIM]
    total = packed[:, QK_DIM + 1, 0]
    top = jnp.where(present, packed[:, QK_DIM + 1, 1], floor_log)
    return (total, memory, normalizer, top)


def entering(state, axis, sign):
    size, mine = lax.axis_size(axis), lax.axis_index(axis)
    place = mine if sign > 0 else size - 1 - mine
    packed = pack(state)
    if size <= 4:
        parts = [unpack(shifted(packed, axis, sign * d), place >= d) for d in range(1, size)]
        result = parts[0]
        for part in parts[1:]:
            result = combine(part, result)
        return result
    result = unpack(shifted(packed, axis, sign), place >= 1)
    reach, step = 1, 1
    while reach < size - 1:
        part = unpack(shifted(pack(result), axis, sign * step), place >= step + 1)
        result = combine(part, result)
        reach += step
        step = reach
    return result


def summarize(keys_scaled, values_wide, in_gate, log_cum, totals):
    growth = totals[:, None] - log_cum + in_gate
    largest = jnp.max(growth, axis=-1)
    weighting = jnp.exp(growth - largest[:, None])
    weighted = keys_scaled * jnp.transpose(weighting)[:, :, None]
    memory = jnp.einsum("shd,she->hde", weighted, values_wide, precision=highest)
    return (totals, memory, jnp.sum(weighted, axis=0), largest)


def own_block(in_gate, log_cum, mask):
    exponent = jnp.where(
        mask[None], log_cum[:, :, None] - log_cum[:, None, :] + in_gate[:, None, :], -jnp.inf
    )
    return exponent, jnp.max(exponent, axis=-1)


def read_out(query_wide, scores, value_heads, exponent, block_top, log_cum, state):
    memory, normalizer, top_in = (state[1], state[2], state[3])
    before = log_cum + top_in[:, None]
    running = jnp.maximum(before, block_top)
    carry_scale = jnp.exp(before - running)
    weights = jnp.exp(exponent - running[:, :, None]) * scores
    numerator = carry_scale[:, :, None] * jnp.einsum(
        "thd,hde->hte", query_wide, memory, precision=highest
    )
    numerator = numerator + jnp.einsum(
        "hts,she->hte",
        weights.astype(jnp.bfloat16),
        value_heads,
        preferred_element_type=jnp.float32,
    )
    denominator = carry_scale * jnp.einsum(
        "thd,hd->ht", query_wide, normalizer, precision=highest
    ) + jnp.sum(weights, axis=-1)
    return numerator / jnp.maximum(jnp.abs(denominator), jnp.exp(-running))[:, :, None]


def heads_part(query, keys, values, out_gate, input_gate, forget_gate, head_gain):
    length = query.shape[0]
    heads_here = input_gate.shape[1]
    query_heads = query.reshape(length, heads_here, QK_DIM)
    keys_heads = keys.reshape(length, heads_here, QK_DIM)
    value_heads = values.reshape(length, heads_here, V_DIM)
    keys_scaled = keys_heads.astype(jnp.float32) * QK_DIM ** (-0.5)
    values_wide = value_heads.astype(jnp.float32)
    query_wide = query_heads.astype(jnp.float32)
    log_keep = jax.nn.log_sigmoid(forget_gate)
    cum_ahead = jnp.cumsum(log_keep[0], axis=-1)
    cum_behind = lax.cumsum(log_keep[1], axis=1, reverse=True)
    ahead = summarize(keys_scaled, values_wide, input_gate[0], cum_ahead, cum_ahead[:, -1])
    behind = summarize(keys_scaled, values_wide, input_gate[1], cum_behind, cum_behind[:, 0])
    ahead_state = entering(ahead, "sp", 1)
    behind_state = entering(behind, "sp", -1)
    scores = jnp.einsum(
        "thd,shd->hts", query_heads, keys_heads, preferred_element_type=jnp.float32
    ) * QK_DIM ** (-0.5)
    lower = jnp.tril(jnp.ones((length, length), dtype=bool))
    both = 0.0
    for way, cum, mask, state in (
        (0, cum_ahead, lower, ahead_state),
        (1, cum_behind, lower.T, behind_state),
    ):
        exponent, block_top = own_block(input_gate[way], cum, mask)
        both = both + read_out(query_wide, scores, value_heads, exponent, block_top, cum, state)
    scaled = both * lax.rsqrt(jnp.mean(both * both, axis=-1, keepdims=True) + epsilon)
    scaled = scaled * head_gain.reshape(heads_here, V_DIM)[:, None, :]
    side_by_side = jnp.transpose(scaled, (1, 0, 2)).reshape(length, heads_here * V_DIM)
    return (side_by_side * jax.nn.sigmoid(out_gate.astype(jnp.float32))).astype(jnp.bfloat16)


def smear(upper, before, after, taps):
    length = upper.shape[1]
    padded = jnp.concatenate([before, upper, after], axis=1)
    total = padded[:, 0:length] * taps[0]
    for offset in range(1, CONV):
        total = total + padded[:, offset : offset + length] * taps[offset]
    return total


def local(
    residual,
    query,
    keys,
    values,
    out_gate,
    input_gate,
    forget_gate,
    head_gain,
    w_out,
    norm_gain,
    w_up_gate,
    w_up_value,
    conv_gate,
    conv_value,
    w_down,
):
    tp, mine = lax.axis_size("tp"), lax.axis_index("tp")
    grp, group = lax.axis_size("grp"), lax.axis_index("grp")
    rows, width = residual.shape
    length = query.shape[0]
    units = w_up_gate.shape[1] // grp

    def unit_share(x, dim):
        return lax.dynamic_slice_in_dim(x, group * units, units, axis=dim)

    gate_whole = lax.all_gather(unit_share(w_up_gate, 1), "sp", axis=0, tiled=True)
    value_whole = lax.all_gather(unit_share(w_up_value, 1), "sp", axis=0, tiled=True)
    down_whole = lax.all_gather(unit_share(w_down, 0), "sp", axis=1, tiled=True)

    w_far = swap(w_out, "tp", 2)
    w_near = swap(w_out, "tp", 1)
    w_pieces = [w_out, w_near, w_far, swap(w_far, "tp", 1)]

    gated = heads_part(query, keys, values, out_gate, input_gate, forget_gate, head_gain)
    blocks = gated.reshape(tp, rows, gated.shape[1])
    projected = jnp.dot(pick(blocks, mine, 0), w_pieces[0], preferred_element_type=jnp.float32)
    for distance in range(1, tp):
        piece = swap(pick(blocks, mine ^ distance, 0), "tp", distance)
        projected = projected + jnp.dot(
            piece, w_pieces[distance], preferred_element_type=jnp.float32
        )
    stream = (residual.astype(jnp.float32) + projected).astype(jnp.bfloat16)
    stream_wide = stream.astype(jnp.float32)
    normed = stream_wide * lax.rsqrt(
        jnp.mean(stream_wide * stream_wide, axis=-1, keepdims=True) + epsilon
    )
    normed = (normed * norm_gain).astype(jnp.bfloat16)

    near, far = mine % 2, mine // 2
    pair = jnp.stack([normed, swap(normed, "grp", 1)], axis=0)
    quad = in_order(pair, swap(pair, "tp", 2), far, 1)
    whole = in_order(quad, swap(quad, "tp", 1), near, 2)
    whole = whole.reshape(grp * length, width)

    def share_up(weight):
        upper = jnp.dot(whole, weight, preferred_element_type=jnp.float32).astype(jnp.bfloat16)
        return upper.reshape(grp, length, units)

    smeared, edges = [], []
    uppers = [share_up(gate_whole), share_up(value_whole)]
    for upper in uppers:
        edges.append((upper[:, -1:], upper[:, :1]))
    last = jnp.concatenate([e[0] for e in edges], axis=-1)
    initial = jnp.concatenate([e[1] for e in edges], axis=-1)
    before = shifted(last, "sp", 1)
    after = shifted(initial, "sp", -1)
    for place, (upper, taps) in enumerate(zip(uppers, (conv_gate, conv_value))):
        cut = slice(place * units, (place + 1) * units)
        smeared.append(smear(upper, before[..., cut], after[..., cut], unit_share(taps, 1)))
    hidden = (jax.nn.silu(smeared[0]) * smeared[1]).astype(jnp.bfloat16)

    hidden = hidden.reshape(grp, tp // 2, 2, rows, units)

    def down(part):
        flat = part.reshape(-1, units)
        terms = jnp.dot(flat, down_whole, preferred_element_type=jnp.float32)
        return terms.reshape(part.shape[:-1] + (width,))

    sent = down(pick(hidden, 1 - near, 2)).astype(jnp.bfloat16)
    got = swap(sent, "tp", 1)
    total = down(pick(hidden, near, 2)) + got.astype(jnp.float32)
    got = swap(pick(total, 1 - far, 1).astype(jnp.bfloat16), "tp", 2)
    total = pick(total, far, 1) + got.astype(jnp.float32)
    got = swap(total[1].astype(jnp.bfloat16), "grp", 1)
    returned = total[0] + got.astype(jnp.float32)
    return (stream_wide + returned).astype(jnp.bfloat16)


def solution(mesh):
    placed = (
        P(("grp", "sp", "tp"), None),
        P(("grp", "sp"), "tp"),
        P(("grp", "sp"), "tp"),
        P(("grp", "sp"), "tp"),
        P(("grp", "sp"), "tp"),
        P(None, "tp", ("grp", "sp")),
        P(None, "tp", ("grp", "sp")),
        P("tp"),
        P("tp", None),
        P(),
        P("sp", "tp"),
        P("sp", "tp"),
        P(None, "tp"),
        P(None, "tp"),
        P("tp", "sp"),
    )
    return jax.shard_map(
        local, mesh=mesh, in_specs=placed, out_specs=P(("grp", "sp", "tp"), None), check_vma=False
    )
```

time: 506 us -> 265 us (0.52)
  waiting for transfers between devices: 347 us -> 129 us
  blocking collectives: 67.9 us -> 0 us
  starting transfers between devices: 2.96 us -> 29.9 us
  loops' own time: 12.3 us -> 0 us
  other arithmetic: 16.1 us -> 24.4 us
  between operations: 13.9 us -> 21.7 us
  matrix products: 25.3 us -> 32.7 us
  local copies, waits for them, and re-layouts: 18.8 us -> 25.9 us
    all_gather x5 -> x3, waiting for transfers between devices: 314 us -> 49.2 us  [the longest x1 37.1 us: local(): down_whole = lax.all_gather(unit_share(w_down, 0), 'sp', axis=1, tiled=True)]
    ppermute x2 -> x20, waiting for transfers between devices: 4.08 us -> 79.5 us  [the longest x12 63.6 us: swap(): return lax.ppermute(x, axis, [(i, i ^ distance) for i in range(size)])]
    all_gather x4 -> x0, blocking collectives: 46.6 us -> none  [entering(): pieces = jax.tree.map(lambda part: lax.all_gather(part, axis), value)]
    ppermute x2 -> x20, starting transfers between devices: 2.76 us -> 29.8 us  [the longest x8 20.3 us: shifted(): return lax.ppermute(x, axis, pairs)]
    reduce_scatter x1 -> x0, waiting for transfers between devices: 26.4 us -> none  [local(): lax.psum_scatter(terms.astype(jnp.bfloat16), 'tp', scatter_dimension=0, t...]
    unnamed x1 -> x0, blocking collectives: 13.5 us -> none
    another operation x2 -> x0, loops' own time: 12.3 us -> none  [entering(): return lax.fori_loop(0, count - 1, step, total)]
    another operation x7 -> x16, other arithmetic: 1.06 us -> 10.5 us  [the longest x4 4.84 us: in_order(): return jnp.stack([first, second], axis=dim)]
  transfers between devices with their start and end apart: 8 -> 23, of which waited for: 6 -> 13; matrix products, arithmetic and copies ran while one was open for 9% -> 25% of each run, Pallas kernels for 0% -> 0%
where the time goes in v1:
time: 265 us; the launch traced here: 263 us
  waiting for transfers between devices  129 us (49%)
  matrix products  32.7 us (12%)
  starting transfers between devices  29.9 us (11%)
  local copies, waits for them, and re-layouts  25.9 us (10%)
  other arithmetic  24.4 us (9%)
  between operations  21.7 us (8%)
    ppermute x12, waiting for transfers between devices, swap(): return lax.ppermute(x, axis, [(i, i ^ distance) for i in range(size)])  63.6 us
    all_gather x1, waiting for transfers between devices, local(): down_whole = lax.all_gather(unit_share(w_down, 0), 'sp', axis=1, tiled=True)  37.1 us
    ppermute x8, starting transfers between devices, shifted(): return lax.ppermute(x, axis, pairs)  20.3 us
    ppermute x8, waiting for transfers between devices, shifted(): return lax.ppermute(x, axis, pairs)  15.9 us
    dot_general x2, matrix products, share_up(): jnp.dot(whole, weight, preferred_element_type=jnp.float32)  12.7 us
    all_gather x1, waiting for transfers between devices, local(): lax.all_gather(unit_share(w_up_value, 1), 'sp', axis=0, tiled=True)  12 us
    ppermute x12, starting transfers between devices, swap(): return lax.ppermute(x, axis, [(i, i ^ distance) for i in range(size)])  9.45 us
    dot_general x2, matrix products, down(): terms = jnp.dot(flat, down_whole, preferred_element_type=jnp.float32)  8.01 us
  transfers between devices with their start and end apart: 23, of which 13 were waited for; matrix products, arithmetic and copies ran while one was open for 25% of the time, Pallas kernels for 0%

profile of v1, /device:TPU:0, one launch (start us, length us, event | category | flops | bytes accessed | tf_op | source)
XLA Modules:
  0.0 263.5 jit_solution(16799234150819835523)
XLA Ops:
  7.9 1.3 constant_dynamic-slice_fusion.4
  13.0 1.8 fusion.75
  14.8 2.5 exponential_multiply_fusion.2
  19.7 6.6 %collective-permute-start.1 = (f32[1,136,256]{2,1,0:T(8,128)}, f32[1,136,256]{2,1,0:T(8,128)}, u32[]{:S(2)}, u32[]{:S(2)}) collective-permute-start(f32[1,136,256]{2,1,0:T(8,128)} %pad_maximum_fusion.7), channel_id=1, source_target_pairs={{0,8},{4,12},{1,9},{5,13},{2,10},{6,14},{3,11},{7,15},{16,24},{20,... | collective-permute-start | bytes 417800 | tf_op jit(solution)/shard_map/ppermute | solution.py:24
  26.4 4.1 %collective-permute-start.2 = (f32[1,136,256]{2,1,0:T(8,128)}, f32[1,136,256]{2,1,0:T(8,128)}, u32[]{:S(2)}, u32[]{:S(2)}) collective-permute-start(f32[1,136,256]{2,1,0:T(8,128)} %pad_maximum_fusion.7), channel_id=1, source_target_pairs={{0,4},{4,8},{8,12},{1,5},{5,9},{9,13},{2,6},{6,10},{10,14},{3,7},{... | collective-permute-start | bytes 417800 | tf_op jit(solution)/shard_map/ppermute | solution.py:24
  30.5 2.0 collective-permute-start
  32.5 1.4 fusion.77
  40.5 1.5 collective-permute-start.3
  41.9 1.4 fusion.104
  43.3 8.4 %collective-permute-done.4 = f32[1,136,256]{2,1,0:T(8,128)} collective-permute-done((f32[1,136,256]{2,1,0:T(8,128)}, f32[1,136,256]{2,1,0:T(8,128)}, u32[]{:S(2)}, u32[]{:S(2)}) %collective-permute-start.4) | collective-permute-done | bytes 139296 | tf_op jit(solution)/shard_map/ppermute | solution.py:24
  51.8 1.4 fusion.102
  53.1 3.2 %collective-permute-done.5 = f32[1,136,256]{2,1,0:T(8,128)} collective-permute-done((f32[1,136,256]{2,1,0:T(8,128)}, f32[1,136,256]{2,1,0:T(8,128)}, u32[]{:S(2)}, u32[]{:S(2)}) %collective-permute-start.5) | collective-permute-done | bytes 139296 | tf_op jit(solution)/shard_map/ppermute | solution.py:24
  56.3 1.5 collective-permute-start.9
  64.1 1.3 fusion.103
  73.7 1.5 fusion.18
  75.2 1.5 multiply_reduce_fusion.1
  76.7 3.3 %collective-permute-done.9 = bf16[256,2048]{1,0:T(8,128)(2,1)} collective-permute-done((bf16[256,2048]{1,0:T(8,128)(2,1)}, bf16[256,2048]{1,0:T(8,128)(2,1)}, u32[]{:S(2)}, u32[]{:S(2)}) %collective-permute-start.9) | collective-permute-done | bytes 1048608 | tf_op jit(solution)/shard_map/ppermute | solution.py:18
  80.9 1.5 fusion.68
  82.4 1.5 collective-permute-start.8
  84.0 1.6 convolution_add_fusion.2
  86.6 1.5 convolution_add_fusion.1
  88.7 1.5 collective-permute-start.12
  90.4 9.3 %collective-permute-done.12 = bf16[96,2048]{1,0:T(8,128)(2,1)S(1)} collective-permute-done((bf16[96,2048]{1,0:T(8,128)(2,1)S(1)}, bf16[96,2048]{1,0:T(8,128)(2,1)S(1)}, u32[]{:S(2)}, u32[]{:S(2)}) %collective-permute-start.12) | collective-permute-done | bytes 393248 | tf_op jit(solution)/shard_map/ppermute | solution.py:18
  101.9 17.4 %collective-permute-done.13 = bf16[2,96,2048]{2,1,0:T(8,128)(2,1)} collective-permute-done((bf16[2,96,2048]{2,1,0:T(8,128)(2,1)}, bf16[2,96,2048]{2,1,0:T(8,128)(2,1)}, u32[]{:S(2)}, u32[]{:S(2)}) %collective-permute-start.13) | collective-permute-done | bytes 786464 | tf_op jit(solution)/shard_map/ppermute | solution.py:18
  119.4 1.3 select_bitcast_fusion.3
  121.6 1.4 pad_maximum_fusion.1
  124.9 1.8 collective-permute-done.14
  126.7 1.8 select_bitcast_fusion.1
  128.8 2.1 copy.27
  131.0 6.4 %convolution_convert_fusion.1 = bf16[768,704]{0,1:T(8,128)(2,1)} fusion(bf16[768,2048]{1,0:T(8,128)(2,1)} %bitcast.198, bf16[2048,704]{1,0:T(8,128)(2,1)} %all-gather.4.cloned.1.call-done), kind=kOutput, calls=%fused_computation.20 | convolution fusion | flops 2215133184 | bytes 7110656 | tf_op jit(solution)/shard_map/dot_general | solution.py:221
  137.3 1.5 copy.46
  138.9 12.0 %all-gather.6.cloned.1.call-done = bf16[2048,704]{1,0:T(8,128)(2,1)} async-done(((bf16[512,704]{1,0:T(8,128)(2,1)}), bf16[2048,704]{1,0:T(8,128)(2,1)}) %all-gather.6.cloned.1.call-update) | async-done | bytes 2883600 | tf_op jit(solution)/shard_map/all_gather | solution.py:192
  150.9 6.3 %convolution_convert_fusion = bf16[768,704]{0,1:T(8,128)(2,1)} fusion(bf16[768,2048]{1,0:T(8,128)(2,1)} %bitcast.199, bf16[2048,704]{1,0:T(8,128)(2,1)} %all-gather.6.cloned.1.call-done), kind=kOutput, calls=%fused_computation.19 | convolution fusion | flops 2215133184 | bytes 7110656 | tf_op jit(solution)/shard_map/dot_general | solution.py:221
  157.3 2.4 copy.47
  160.5 2.1 collective-permute-start.15
  162.7 1.5 collective-permute-start.16
  164.3 4.3 %collective-permute-done.16 = bf16[2,1,1408]{2,1,0:T(2,128)(2,1)S(1)} collective-permute-done((bf16[2,1,1408]{2,1,0:T(2,128)(2,1)S(1)}, bf16[2,1,1408]{2,1,0:T(2,128)(2,1)S(1)}, u32[]{:S(2)}, u32[]{:S(2)}) %collective-permute-start.16) | collective-permute-done | bytes 5664 | tf_op jit(solution)/shard_map/ppermute | solution.py:24
  168.7 4.5 %multiply_convert_fusion = bf16[2,384,704]{2,1,0:T(8,128)(2,1)S(1)} fusion(bf16[2,384,704]{2,1,0:T(8,128)(2,1)} %bitcast.196, bf16[2,384,704]{2,1,0:T(8,128)(2,1)S(1)} %bitcast.194, bf16[2,1,704]{2,1,0:T(2,128)(2,1)S(1)} %get-tuple-element.53, bf16[2,1,704]{2,1,0:T(2,128)(2,1)S(1)} %get-tuple-element.51, bf16[2,1,704]{2,1,0:T(2,128)(2,1)S(1)} %get-tuple-element.52, ...), kind=kLoop, calls=%fused_computation.11 | loop fusion | flops 18382848 | bytes 3272192 | tf_op jit(solution)/shard_map/convert_element_type | solution.py:235
  173.3 37.1 %all-gather.8.cloned.1.call-done = bf16[704,2048]{1,0:T(8,128)(2,1)} async-done(((bf16[704,512]{1,0:T(8,128)(2,1)}), bf16[704,2048]{1,0:T(8,128)(2,1)}) %all-gather.8.cloned.1.call-update) | async-done | bytes 2883600 | tf_op jit(solution)/shard_map/all_gather | solution.py:193
  210.5 4.3 %fusion.6 = bf16[2,2,96,2048]{3,2,0,1:T(8,128)(2,1)} fusion(bf16[704,2048]{1,0:T(8,128)(2,1)} %all-gather.8.cloned.1.call-done, bf16[2,2,96,704]{3,2,1,0:T(8,128)(2,1)S(1)} %get-tuple-element.34), kind=kOutput, calls=%fused_computation.6 | convolution fusion | flops 1108082688 | bytes 4997120 | tf_op jit(solution)/shard_map/dot_general | solution.py:241
  214.8 3.7 %collective-permute-done.17 = bf16[2,2,96,2048]{3,2,0,1:T(8,128)(2,1)} collective-permute-done((bf16[2,2,96,2048]{3,2,0,1:T(8,128)(2,1)}, bf16[2,2,96,2048]{3,2,0,1:T(8,128)(2,1)}, u32[]{:S(2)}, u32[]{:S(2)}) %collective-permute-start.17) | collective-permute-done | bytes 1572896 | tf_op jit(solution)/shard_map/ppermute | solution.py:18
  218.6 3.7 %convert_add_fusion = f32[2,2,96,2048]{3,2,0,1:T(8,128)S(1)} fusion(bf16[2,2,96,2048]{3,2,0,1:T(8,128)(2,1)} %collective-permute-done.17, bf16[704,2048]{1,0:T(8,128)(2,1)} %all-gather.8.cloned.1.call-done, bf16[2,2,96,704]{3,2,1,0:T(8,128)(2,1)S(1)} %get-tuple-element.33), kind=kOutput, calls=%fused_computation.1 | convolution fusion | flops 1108869120 | bytes 8142848 | tf_op jit(solution)/shard_map/dot_general | solution.py:241
  222.3 1.7 copy-done.2
  224.0 1.5 collective-permute-start.18
  225.6 18.2 %collective-permute-done.18 = bf16[2,96,2048]{2,1,0:T(8,128)(2,1)} collective-permute-done((bf16[2,96,2048]{2,1,0:T(8,128)(2,1)S(1)}, bf16[2,96,2048]{2,1,0:T(8,128)(2,1)}, u32[]{:S(2)}, u32[]{:S(2)}) %collective-permute-start.18) | collective-permute-done | bytes 786464 | tf_op jit(solution)/shard_map/ppermute | solution.py:18
  243.8 1.8 bitcast_add_fusion
  245.7 1.5 collective-permute-start.19
  247.2 8.8 %collective-permute-done.19 = bf16[96,2048]{1,0:T(8,128)(2,1)S(1)} collective-permute-done((bf16[96,2048]{1,0:T(8,128)(2,1)S(1)}, bf16[96,2048]{1,0:T(8,128)(2,1)S(1)}, u32[]{:S(2)}, u32[]{:S(2)}) %collective-permute-start.19) | collective-permute-done | bytes 393248 | tf_op jit(solution)/shard_map/ppermute | solution.py:18
  (118 shorter events, 30.7 us)
Async XLA Ops:
  6.5 1.4 copy-start
  6.5 2.8 %copy-start.12 = (f32[2,1,384]{2,1,0:T(1,128)S(1)}, f32[2,1,384]{2,1,0:T(1,128)}, u32[]{:S(2)}) copy-start(f32[2,1,384]{2,1,0:T(1,128)} %param.21) | copy-start | bytes 9220
  6.5 6.4 %copy-start.11 = (f32[2,1,384]{2,1,0:T(1,128)S(1)}, f32[2,1,384]{2,1,0:T(1,128)}, u32[]{:S(2)}) copy-start(f32[2,1,384]{2,1,0:T(1,128)} %param.20) | copy-start | bytes 9220
  6.5 10.7 %copy-start.4 = (bf16[384,128]{1,0:T(8,128)(2,1)S(1)}, bf16[384,128]{1,0:T(8,128)(2,1)}, u32[]{:S(2)}) copy-start(bf16[384,128]{1,0:T(8,128)(2,1)} %param.17) | copy-start | bytes 294916
  6.5 12.1 %copy-start.5 = (bf16[384,256]{1,0:T(8,128)(2,1)S(1)}, bf16[384,256]{1,0:T(8,128)(2,1)}, u32[]{:S(2)}) copy-start(bf16[384,256]{1,0:T(8,128)(2,1)} %param.18) | copy-start | bytes 589828
  6.5 31.0 %copy-start.6 = (bf16[512,1408]{1,0:T(8,128)(2,1)S(1)}, bf16[512,1408]{1,0:T(8,128)(2,1)}, u32[]{:S(2)}) copy-start(bf16[512,1408]{1,0:T(8,128)(2,1)} %param.26) | copy-start | bytes 4325380
  6.6 124.4 %all-gather.4.cloned.1.call-start = ((), (), s32[]{:S(2)}) async-start(), calls=%async_computation | async-start | bytes 3932160 | tf_op jit(solution)/shard_map/all_gather | solution.py:191
  9.3 60.9 %copy-start.8 = (bf16[384,128]{1,0:T(8,128)(2,1)S(1)}, bf16[384,128]{1,0:T(8,128)(2,1)}, u32[]{:S(2)}) copy-start(bf16[384,128]{1,0:T(8,128)(2,1)} %param.16) | copy-start | bytes 294916
  9.3 141.7 %all-gather.6.cloned.1.call-start = ((), (), s32[]{:S(2)}) async-start(), calls=%async_computation.1 | async-start | bytes 3932160 | tf_op jit(solution)/shard_map/all_gather | solution.py:192
  19.7 20.7 %collective-permute-start.1 = (f32[1,136,256]{2,1,0:T(8,128)}, f32[1,136,256]{2,1,0:T(8,128)}, u32[]{:S(2)}, u32[]{:S(2)}) collective-permute-start(f32[1,136,256]{2,1,0:T(8,128)} %pad_maximum_fusion.7), channel_id=1, source_target_pairs={{0,8},{4,12},{1,9},{5,13},{2,10},{6,14},{3,11},{7,15},{16,24},{20,... | collective-permute-start | bytes 417800 | tf_op jit(solution)/shard_map/ppermute | solution.py:24
  26.4 37.7 %collective-permute-start.2 = (f32[1,136,256]{2,1,0:T(8,128)}, f32[1,136,256]{2,1,0:T(8,128)}, u32[]{:S(2)}, u32[]{:S(2)}) collective-permute-start(f32[1,136,256]{2,1,0:T(8,128)} %pad_maximum_fusion.7), channel_id=1, source_target_pairs={{0,4},{4,8},{8,12},{1,5},{5,9},{9,13},{2,6},{6,10},{10,14},{3,7},{... | collective-permute-start | bytes 417800 | tf_op jit(solution)/shard_map/ppermute | solution.py:24
  30.5 37.5 %collective-permute-start = (f32[1,136,256]{2,1,0:T(8,128)}, f32[1,136,256]{2,1,0:T(8,128)}, u32[]{:S(2)}, u32[]{:S(2)}) collective-permute-start(f32[1,136,256]{2,1,0:T(8,128)} %pad_maximum_fusion.7), channel_id=1, source_target_pairs={{0,12},{1,13},{2,14},{3,15},{16,28},{17,29},{18,30},{19,31}} | collective-permute-start | bytes 417800 | tf_op jit(solution)/shard_map/ppermute | solution.py:24
  34.9 16.8 %collective-permute-start.4 = (f32[1,136,256]{2,1,0:T(8,128)}, f32[1,136,256]{2,1,0:T(8,128)}, u32[]{:S(2)}, u32[]{:S(2)}) collective-permute-start(f32[1,136,256]{2,1,0:T(8,128)} %pad_maximum_fusion.8), channel_id=1, source_target_pairs={{8,0},{12,4},{9,1},{13,5},{10,2},{14,6},{11,3},{15,7},{24,16},{28,... | collective-permute-start | bytes 417800 | tf_op jit(solution)/shard_map/ppermute | solution.py:24
  36.2 20.1 %collective-permute-start.5 = (f32[1,136,256]{2,1,0:T(8,128)}, f32[1,136,256]{2,1,0:T(8,128)}, u32[]{:S(2)}, u32[]{:S(2)}) collective-permute-start(f32[1,136,256]{2,1,0:T(8,128)} %pad_maximum_fusion.8), channel_id=1, source_target_pairs={{4,0},{8,4},{12,8},{5,1},{9,5},{13,9},{6,2},{10,6},{14,10},{7,3},{... | collective-permute-start | bytes 417800 | tf_op jit(solution)/shard_map/ppermute | solution.py:24
  38.9 171.6 %all-gather.8.cloned.1.call-start = ((), (), s32[]{:S(2)}) async-start(), calls=%async_computation.2 | async-start | bytes 3604480 | tf_op jit(solution)/shard_map/all_gather | solution.py:193
  40.5 21.7 %collective-permute-start.3 = (f32[1,136,256]{2,1,0:T(8,128)}, f32[1,136,256]{2,1,0:T(8,128)S(1)}, u32[]{:S(2)}, u32[]{:S(2)}) collective-permute-start(f32[1,136,256]{2,1,0:T(8,128)} %pad_maximum_fusion.8), channel_id=1, source_target_pairs={{12,0},{13,1},{14,2},{15,3},{28,16},{29,17},{30,18},{31,19}} | collective-permute-start | bytes 417800 | tf_op jit(solution)/shard_map/ppermute | solution.py:24
  51.7 32.2 %collective-permute-start.7 = (bf16[256,2048]{1,0:T(8,128)(2,1)}, bf16[256,2048]{1,0:T(8,128)(2,1)}, u32[]{:S(2)}, u32[]{:S(2)}) collective-permute-start(bf16[256,2048]{1,0:T(8,128)(2,1)} %param.23), channel_id=1, source_target_pairs={{0,1},{1,0},{2,3},{3,2},{4,5},{5,4},{6,7},{7,6},{8,9},{9,8},{10,11... | collective-permute-start | bytes 3145736 | tf_op jit(solution)/shard_map/ppermute | solution.py:18
  56.3 23.7 %collective-permute-start.9 = (bf16[256,2048]{1,0:T(8,128)(2,1)}, bf16[256,2048]{1,0:T(8,128)(2,1)}, u32[]{:S(2)}, u32[]{:S(2)}) collective-permute-start(bf16[256,2048]{1,0:T(8,128)(2,1)} %param.23), channel_id=1, source_target_pairs={{0,2},{1,3},{2,0},{3,1},{4,6},{5,7},{6,4},{7,5},{8,10},{9,11},{10,... | collective-permute-start | bytes 3145736 | tf_op jit(solution)/shard_map/ppermute | solution.py:18
  73.2 6.8 %copy-start.13 = (f32[256]{0:T(256)S(1)}, f32[256]{0:T(256)}, u32[]{:S(2)}) copy-start(f32[256]{0:T(256)} %param.22) | copy-start | bytes 3076
  80.0 8.1 %collective-permute-start.11 = (bf16[256,2048]{1,0:T(8,128)(2,1)}, bf16[256,2048]{1,0:T(8,128)(2,1)S(1)}, u32[]{:S(2)}, u32[]{:S(2)}) collective-permute-start(bf16[256,2048]{1,0:T(8,128)(2,1)} %collective-permute-done.9), channel_id=1, source_target_pairs={{0,1},{1,0},{2,3},{3,2},{4,5},{5,4},{6,7},{7,6},{8,9},{9,8},{10,11... | collective-permute-start | bytes 3145736 | tf_op jit(solution)/shard_map/ppermute | solution.py:18
  80.3 3.6 %collective-permute-start.6 = (bf16[96,256]{1,0:T(8,128)(2,1)S(1)}, bf16[96,256]{1,0:T(8,128)(2,1)S(1)}, u32[]{:S(2)}, u32[]{:S(2)}) collective-permute-start(bf16[96,256]{1,0:T(8,128)(2,1)S(1)} %get-tuple-element.41), channel_id=1, source_target_pairs={{0,1},{1,0},{2,3},{3,2},{4,5},{5,4},{6,7},{7,6},{8,9},{9,8},{10,11... | collective-permute-start | bytes 147464 | tf_op jit(solution)/shard_map/ppermute | solution.py:18
  82.4 4.2 %collective-permute-start.8 = (bf16[96,256]{1,0:T(8,128)(2,1)S(1)}, bf16[96,256]{1,0:T(8,128)(2,1)S(1)}, u32[]{:S(2)}, u32[]{:S(2)}) collective-permute-start(bf16[96,256]{1,0:T(8,128)(2,1)S(1)} %get-tuple-element.40), channel_id=1, source_target_pairs={{0,2},{1,3},{2,0},{3,1},{4,6},{5,7},{6,4},{7,5},{8,10},{9,11},{10,... | collective-permute-start | bytes 147464 | tf_op jit(solution)/shard_map/ppermute | solution.py:18
  84.0 4.2 %copy-start.7 = (bf16[96,2048]{1,0:T(8,128)(2,1)S(1)}, bf16[96,2048]{1,0:T(8,128)(2,1)}, u32[]{:S(2)}) copy-start(bf16[96,2048]{1,0:T(8,128)(2,1)} %param.15) | copy-start | bytes 1179652
  84.0 4.1 %collective-permute-start.10 = (bf16[96,256]{1,0:T(8,128)(2,1)S(1)}, bf16[96,256]{1,0:T(8,128)(2,1)S(1)}, u32[]{:S(2)}, u32[]{:S(2)}) collective-permute-start(bf16[96,256]{1,0:T(8,128)(2,1)S(1)} %get-tuple-element.39), channel_id=1, source_target_pairs={{0,3},{1,2},{2,1},{3,0},{4,7},{5,6},{6,5},{7,4},{8,11},{9,10},{10,... | collective-permute-start | bytes 147464 | tf_op jit(solution)/shard_map/ppermute | solution.py:18
  85.6 3.0 %copy-start.10 = (f32[2048]{0:T(1024)S(1)}, f32[2048]{0:T(1024)}, u32[]{:S(2)}) copy-start(f32[2048]{0:T(1024)} %param.24) | copy-start | bytes 24580
  88.7 10.9 %collective-permute-start.12 = (bf16[96,2048]{1,0:T(8,128)(2,1)S(1)}, bf16[96,2048]{1,0:T(8,128)(2,1)S(1)}, u32[]{:S(2)}, u32[]{:S(2)}) collective-permute-start(bf16[96,2048]{1,0:T(8,128)(2,1)S(1)} %multiply_convert_fusion.1), channel_id=1, source_target_pairs={{0,16},{16,0},{1,17},{17,1},{2,18},{18,2},{3,19},{19,3},{4,20},{20... | collective-permute-start | bytes 1179656 | tf_op jit(solution)/shard_map/ppermute | solution.py:18
  99.6 2.3 copy-start.3
  100.6 18.7 %collective-permute-start.13 = (bf16[2,96,2048]{2,1,0:T(8,128)(2,1)}, bf16[2,96,2048]{2,1,0:T(8,128)(2,1)}, u32[]{:S(2)}, u32[]{:S(2)}) collective-permute-start(bf16[2,96,2048]{2,1,0:T(8,128)(2,1)} %pad_maximum_fusion.6), channel_id=1, source_target_pairs={{0,2},{1,3},{2,0},{3,1},{4,6},{5,7},{6,4},{7,5},{8,10},{9,11},{10,... | collective-permute-start | bytes 2359304 | tf_op jit(solution)/shard_map/ppermute | solution.py:18
  120.7 0.9 copy-start.1
  120.7 2.2 copy-start.9
  122.9 3.8 %collective-permute-start.14 = (bf16[2,2,96,2048]{3,2,0,1:T(8,128)(2,1)}, bf16[2,2,96,2048]{3,2,0,1:T(8,128)(2,1)}, u32[]{:S(2)}, u32[]{:S(2)}) collective-permute-start(bf16[2,2,96,2048]{3,2,0,1:T(8,128)(2,1)} %pad_maximum_fusion.1), channel_id=1, source_target_pairs={{0,1},{1,0},{2,3},{3,2},{4,5},{5,4},{6,7},{7,6},{8,9},{9,8},{10,11... | collective-permute-start | bytes 4718600 | tf_op jit(solution)/shard_map/ppermute | solution.py:18
  160.5 3.7 %collective-permute-start.15 = (bf16[2,1,1408]{2,1,0:T(2,128)(2,1)S(1)}, bf16[2,1,1408]{2,1,0:T(2,128)(2,1)S(1)}, u32[]{:S(2)}, u32[]{:S(2)}) collective-permute-start(bf16[2,1,1408]{2,1,0:T(2,128)(2,1)S(1)} %pad_maximum_fusion.9), channel_id=1, source_target_pairs={{0,4},{4,8},{8,12},{1,5},{5,9},{9,13},{2,6},{6,10},{10,14},{3,7},{... | collective-permute-start | bytes 16904 | tf_op jit(solution)/shard_map/ppermute | solution.py:24
  162.7 5.9 %collective-permute-start.16 = (bf16[2,1,1408]{2,1,0:T(2,128)(2,1)S(1)}, bf16[2,1,1408]{2,1,0:T(2,128)(2,1)S(1)}, u32[]{:S(2)}, u32[]{:S(2)}) collective-permute-start(bf16[2,1,1408]{2,1,0:T(2,128)(2,1)S(1)} %pad_maximum_fusion.10), channel_id=1, source_target_pairs={{4,0},{8,4},{12,8},{5,1},{9,5},{13,9},{6,2},{10,6},{14,10},{7,3},{... | collective-permute-start | bytes 16904 | tf_op jit(solution)/shard_map/ppermute | solution.py:24
  214.8 3.8 %collective-permute-start.17 = (bf16[2,2,96,2048]{3,2,0,1:T(8,128)(2,1)}, bf16[2,2,96,2048]{3,2,0,1:T(8,128)(2,1)}, u32[]{:S(2)}, u32[]{:S(2)}) collective-permute-start(bf16[2,2,96,2048]{3,2,0,1:T(8,128)(2,1)} %fusion.6), channel_id=1, source_target_pairs={{0,1},{1,0},{2,3},{3,2},{4,5},{5,4},{6,7},{7,6},{8,9},{9,8},{10,11... | collective-permute-start | bytes 4718600 | tf_op jit(solution)/shard_map/ppermute | solution.py:18
  222.3 1.7 copy-start.2
  224.0 19.8 %collective-permute-start.18 = (bf16[2,96,2048]{2,1,0:T(8,128)(2,1)S(1)}, bf16[2,96,2048]{2,1,0:T(8,128)(2,1)}, u32[]{:S(2)}, u32[]{:S(2)}) collective-permute-start(bf16[2,96,2048]{2,1,0:T(8,128)(2,1)S(1)} %fusion.19), channel_id=1, source_target_pairs={{0,2},{1,3},{2,0},{3,1},{4,6},{5,7},{6,4},{7,5},{8,10},{9,11},{10,... | collective-permute-start | bytes 2359304 | tf_op jit(solution)/shard_map/ppermute | solution.py:18
  245.7 10.4 %collective-permute-start.19 = (bf16[96,2048]{1,0:T(8,128)(2,1)S(1)}, bf16[96,2048]{1,0:T(8,128)(2,1)S(1)}, u32[]{:S(2)}, u32[]{:S(2)}) collective-permute-start(bf16[96,2048]{1,0:T(8,128)(2,1)S(1)} %fusion.27), channel_id=1, source_target_pairs={{0,16},{16,0},{1,17},{17,1},{2,18},{18,2},{3,19},{19,3},{4,20},{20... | collective-permute-start | bytes 1179656 | tf_op jit(solution)/shard_map/ppermute | solution.py:18
Sparse Core Ops, SparseCore 0:
  9.4 77.8 all-gather.3
  88.9 62.0 all-gather.5
  152.5 57.9 all-gather.7

commit v2 on v1

--- a/solution.py
+++ b/solution.py
@@ -66,20 +66,13 @@
 def entering(state, axis, sign):
     size, mine = lax.axis_size(axis), lax.axis_index(axis)
     place = mine if sign > 0 else size - 1 - mine
-    packed = pack(state)
-    if size <= 4:
-        parts = [unpack(shifted(packed, axis, sign * d), place >= d) for d in range(1, size)]
-        result = parts[0]
-        for part in parts[1:]:
-            result = combine(part, result)
-        return result
-    result = unpack(shifted(packed, axis, sign), place >= 1)
-    reach, step = 1, 1
-    while reach < size - 1:
-        part = unpack(shifted(pack(result), axis, sign * step), place >= step + 1)
-        result = combine(part, result)
-        reach += step
-        step = reach
+    window, result, step = state, None, 1
+    while step < size:
+        got = unpack(shifted(pack(window), axis, sign * step), place >= step)
+        result = got if result is None else combine(got, result)
+        step *= 2
+        if step < size:
+            window = combine(got, window)
     return result
 
 
@@ -188,8 +181,8 @@
     def unit_share(x, dim):
         return lax.dynamic_slice_in_dim(x, group * units, units, axis=dim)
 
-    gate_whole = lax.all_gather(unit_share(w_up_gate, 1), "sp", axis=0, tiled=True)
-    value_whole = lax.all_gather(unit_share(w_up_value, 1), "sp", axis=0, tiled=True)
+    up_share = jnp.concatenate([unit_share(w_up_gate, 1), unit_share(w_up_value, 1)], axis=1)
+    up_whole = lax.all_gather(up_share, "sp", axis=0, tiled=True)
     down_whole = lax.all_gather(unit_share(w_down, 0), "sp", axis=1, tiled=True)
 
     w_far = swap(w_out, "tp", 2)
@@ -217,37 +210,38 @@
     whole = in_order(quad, swap(quad, "tp", 1), near, 2)
     whole = whole.reshape(grp * length, width)
 
-    def share_up(weight):
-        upper = jnp.dot(whole, weight, preferred_element_type=jnp.float32).astype(jnp.bfloat16)
-        return upper.reshape(grp, length, units)
-
-    smeared, edges = [], []
-    uppers = [share_up(gate_whole), share_up(value_whole)]
-    for upper in uppers:
-        edges.append((upper[:, -1:], upper[:, :1]))
-    last = jnp.concatenate([e[0] for e in edges], axis=-1)
-    initial = jnp.concatenate([e[1] for e in edges], axis=-1)
-    before = shifted(last, "sp", 1)
-    after = shifted(initial, "sp", -1)
-    for place, (upper, taps) in enumerate(zip(uppers, (conv_gate, conv_value))):
-        cut = slice(place * units, (place + 1) * units)
-        smeared.append(smear(upper, before[..., cut], after[..., cut], unit_share(taps, 1)))
-    hidden = (jax.nn.silu(smeared[0]) * smeared[1]).astype(jnp.bfloat16)
+    upper = jnp.dot(whole, up_whole, preferred_element_type=jnp.float32).astype(jnp.bfloat16)
+    upper = upper.reshape(grp, length, 2 * units)
+    taps = jnp.concatenate([unit_share(conv_gate, 1), unit_share(conv_value, 1)], axis=1)
+    before = shifted(upper[:, -1:], "sp", 1)
+    after = shifted(upper[:, :1], "sp", -1)
+    smeared = smear(upper, before, after, taps)
+    hidden = (jax.nn.silu(smeared[..., :units]) * smeared[..., units:]).astype(jnp.bfloat16)
 
     hidden = hidden.reshape(grp, tp // 2, 2, rows, units)
-
-    def down(part):
-        flat = part.reshape(-1, units)
-        terms = jnp.dot(flat, down_whole, preferred_element_type=jnp.float32)
-        return terms.reshape(part.shape[:-1] + (width,))
-
-    sent = down(pick(hidden, 1 - near, 2)).astype(jnp.bfloat16)
-    got = swap(sent, "tp", 1)
-    total = down(pick(hidden, near, 2)) + got.astype(jnp.float32)
-    got = swap(pick(total, 1 - far, 1).astype(jnp.bfloat16), "tp", 2)
-    total = pick(total, far, 1) + got.astype(jnp.float32)
-    got = swap(total[1].astype(jnp.bfloat16), "grp", 1)
-    returned = total[0] + got.astype(jnp.float32)
+    hidden_sent = pick(hidden, 1 - near, 2).reshape(-1, units)
+    hidden_kept = pick(hidden, near, 2).reshape(-1, units)
+    halves = (down_whole[:, : width // 2], down_whole[:, width // 2 :])
+
+    def down(part, weight):
+        terms = jnp.dot(part, weight, preferred_element_type=jnp.float32)
+        return terms.reshape(grp, tp // 2, rows, width // 2)
+
+    def over_far(total, dim):
+        got = swap(pick(total, 1 - far, dim).astype(jnp.bfloat16), "tp", 2)
+        return pick(total, far, dim) + got.astype(jnp.float32)
+
+    def over_group(total):
+        got = swap(total[1].astype(jnp.bfloat16), "grp", 1)
+        return total[0] + got.astype(jnp.float32)
+
+    gots = [swap(down(hidden_sent, half).astype(jnp.bfloat16), "tp", 1) for half in halves]
+    totals = [
+        down(hidden_kept, half) + got.astype(jnp.float32) for half, got in zip(halves, gots)
+    ]
+    first = over_group(over_far(totals[0], 1))
+    second = over_far(over_group(totals[1]), 0)
+    returned = jnp.concatenate([first, second], axis=1)
     return (stream_wide + returned).astype(jnp.bfloat16)
 
 

time: 265 us -> 247 us (0.932)
  local copies, waits for them, and re-layouts: 25.9 us -> 14.4 us
  waiting for transfers between devices: 129 us -> 118 us
  other arithmetic: 24.4 us -> 29.8 us
    ppermute x12 -> x15, waiting for transfers between devices: 63.6 us -> 44.8 us  [swap(): return lax.ppermute(x, axis, [(i, i ^ distance) for i in range(size)])]
    ppermute x8 -> x6, waiting for transfers between devices: 15.9 us -> 23 us  [shifted(): return lax.ppermute(x, axis, pairs)]
    add x1 -> x9, other arithmetic: 1.83 us -> 8.46 us  [the longest x1 4.89 us: smear(): total = total + padded[:, offset:offset + length] * taps[offset]]
    slice x6 -> x2, local copies, waits for them, and re-layouts: 7.37 us -> 1.14 us  [unpack(): top = jnp.where(present, packed[:, QK_DIM + 1, 1], floor_log)]
    ppermute x8 -> x6, starting transfers between devices: 20.3 us -> 14.7 us  [shifted(): return lax.ppermute(x, axis, pairs)]
    reshape x2 -> x0, local copies, waits for them, and re-layouts: 3.93 us -> none  [share_up(): return upper.reshape(grp, length, units)]
    ppermute x12 -> x15, starting transfers between devices: 9.45 us -> 13.3 us  [swap(): return lax.ppermute(x, axis, [(i, i ^ distance) for i in range(size)])]
    convert_element_type x1, other arithmetic: 4.54 us -> 0.71 us  [local(): (jax.nn.silu(smeared[..., :units]) * smeared[..., units:]).astype(jnp.bfl...]
  transfers between devices with their start and end apart: 23 -> 23, of which waited for: 13 -> 13; matrix products, arithmetic and copies ran while one was open for 25% -> 28% of each run, Pallas kernels for 0% -> 0%
where the time goes in v2:
time: 247 us; the launch traced here: 245 us
  waiting for transfers between devices  118 us (48%)
  matrix products  31.2 us (13%)
  other arithmetic  29.8 us (12%)
  starting transfers between devices  28.1 us (11%)
  between operations  24.1 us (10%)
  local copies, waits for them, and re-layouts  14.4 us (6%)
    ppermute x15, waiting for transfers between devices, swap(): return lax.ppermute(x, axis, [(i, i ^ distance) for i in range(size)])  44.8 us
    all_gather x1, waiting for transfers between devices, local(): down_whole = lax.all_gather(unit_share(w_down, 0), 'sp', axis=1, tiled=True)  36.3 us
    ppermute x6, waiting for transfers between devices, shifted(): return lax.ppermute(x, axis, pairs)  23 us
    ppermute x6, starting transfers between devices, shifted(): return lax.ppermute(x, axis, pairs)  14.7 us
    all_gather x1, waiting for transfers between devices, local(): up_whole = lax.all_gather(up_share, 'sp', axis=0, tiled=True)  13.7 us
    ppermute x15, starting transfers between devices, swap(): return lax.ppermute(x, axis, [(i, i ^ distance) for i in range(size)])  13.3 us
    dot_general x4, matrix products, down(): terms = jnp.dot(part, weight, preferred_element_type=jnp.float32)  9.09 us
    dot_general x1, matrix products, local(): jnp.dot(whole, up_whole, preferred_element_type=jnp.float32)  8.35 us
  transfers between devices with their start and end apart: 23, of which 13 were waited for; matrix products, arithmetic and copies ran while one was open for 28% of the time, Pallas kernels for 0%

profile of v2, /device:TPU:0, one launch (start us, length us, event | category | flops | bytes accessed | tf_op | source)
XLA Modules:
  0.0 245.5 jit_solution(13333052185417633173)
XLA Ops:
  7.0 2.6 %collective-permute-start.7 = (bf16[256,2048]{1,0:T(8,128)(2,1)}, bf16[256,2048]{1,0:T(8,128)(2,1)}, u32[]{:S(2)}, u32[]{:S(2)}) collective-permute-start(bf16[256,2048]{1,0:T(8,128)(2,1)} %param.23), channel_id=1, source_target_pairs={{0,2},{1,3},{2,0},{3,1},{4,6},{5,7},{6,4},{7,5},{8,10},{9,11},{10,... | collective-permute-start | bytes 3145736 | tf_op jit(solution)/shard_map/ppermute | solution.py:18
  14.6 2.5 %fusion.68 = (f32[]{:T(128)}, f32[]{:T(128)}) fusion(f32[1,384]{1,0:T(1,128)S(1)} %bitcast_add_fusion.6, f32[2,1,384]{2,1,0:T(1,128)} %param.20, f32[]{:T(128)} %bitcast.37, f32[1,384]{1,0:T(1,128)S(1)} %bitcast_add_fusion.7, f32[]{:T(128)} %bitcast.5), kind=kLoop, calls=%fused_computation.157 | loop fusion | flops 2302 | bytes 6160 | tf_op jit(solution)/shard_map/reduce_max | solution.py:81
  17.1 2.5 exponential_multiply_fusion.2
  21.9 1.4 fusion.41
  23.4 4.1 %collective-permute-start = (f32[1,136,256]{2,1,0:T(8,128)S(1)}, f32[1,136,256]{2,1,0:T(8,128)}, u32[]{:S(2)}, u32[]{:S(2)}) collective-permute-start(f32[1,136,256]{2,1,0:T(8,128)S(1)} %pad_maximum_fusion.6), channel_id=1, source_target_pairs={{0,4},{4,8},{8,12},{1,5},{5,9},{9,13},{2,6},{6,10},{10,14},{3,7},{... | collective-permute-start | bytes 417800 | tf_op jit(solution)/shard_map/ppermute | solution.py:24
  27.5 1.4 fusion.43
  30.2 1.3 collective-permute-start.2
  31.6 1.9 constant_dynamic-slice_fusion.3
  33.5 1.6 pad_maximum_fusion.4
  35.2 1.4 fusion.90
  38.9 1.3 fusion.89
  45.7 5.0 %collective-permute-start.1 = (f32[1,136,256]{2,1,0:T(8,128)S(1)}, f32[1,136,256]{2,1,0:T(8,128)S(1)}, u32[]{:S(2)}, u32[]{:S(2)}) collective-permute-start(f32[1,136,256]{2,1,0:T(8,128)S(1)} %pad_maximum_fusion.7), channel_id=1, source_target_pairs={{0,8},{4,12},{1,9},{5,13},{2,10},{6,14},{3,11},{7,15},{16,24},{20,... | collective-permute-start | bytes 417800 | tf_op jit(solution)/shard_map/ppermute | solution.py:24
  53.8 1.5 collective-permute-start.3
  55.9 18.7 %collective-permute-done.3 = f32[1,136,256]{2,1,0:T(8,128)S(1)} collective-permute-done((f32[1,136,256]{2,1,0:T(8,128)S(1)}, f32[1,136,256]{2,1,0:T(8,128)S(1)}, u32[]{:S(2)}, u32[]{:S(2)}) %collective-permute-start.3) | collective-permute-done | bytes 139296 | tf_op jit(solution)/shard_map/ppermute | solution.py:24
  81.2 1.3 fusion.10
  83.1 1.4 multiply_reduce_fusion.1
  85.4 1.5 fusion.62
  87.0 1.4 collective-permute-start.6
  88.6 1.5 convolution_add_fusion.2
  91.1 1.5 convolution_add_fusion.1
  93.5 1.5 collective-permute-start.10
  95.2 9.0 %collective-permute-done.10 = bf16[96,2048]{1,0:T(8,128)(2,1)S(1)} collective-permute-done((bf16[96,2048]{1,0:T(8,128)(2,1)S(1)}, bf16[96,2048]{1,0:T(8,128)(2,1)S(1)}, u32[]{:S(2)}, u32[]{:S(2)}) %collective-permute-start.10) | collective-permute-done | bytes 393248 | tf_op jit(solution)/shard_map/ppermute | solution.py:18
  105.2 1.3 collective-permute-start.11
  106.5 17.3 %collective-permute-done.11 = bf16[2,96,2048]{2,1,0:T(8,128)(2,1)} collective-permute-done((bf16[2,96,2048]{2,1,0:T(8,128)(2,1)}, bf16[2,96,2048]{2,1,0:T(8,128)(2,1)}, u32[]{:S(2)}, u32[]{:S(2)}) %collective-permute-start.11) | collective-permute-done | bytes 786464 | tf_op jit(solution)/shard_map/ppermute | solution.py:18
  123.8 1.4 select_bitcast_fusion.3
  126.1 1.4 pad_maximum_fusion.3
  128.4 2.8 %collective-permute-done.12 = bf16[2,2,96,2048]{3,2,0,1:T(8,128)(2,1)} collective-permute-done((bf16[2,2,96,2048]{3,2,0,1:T(8,128)(2,1)}, bf16[2,2,96,2048]{3,2,0,1:T(8,128)(2,1)}, u32[]{:S(2)}, u32[]{:S(2)}) %collective-permute-start.12) | collective-permute-done | bytes 1572896 | tf_op jit(solution)/shard_map/ppermute | solution.py:18
  131.2 1.8 select_bitcast_fusion.1
  133.3 2.1 copy.27
  135.4 13.7 %all-gather.3.cloned.1.call-done = bf16[2048,1408]{1,0:T(8,128)(2,1)} async-done(((bf16[512,1408]{1,0:T(8,128)(2,1)}), bf16[2048,1408]{1,0:T(8,128)(2,1)}) %all-gather.3.cloned.1.call-update) | async-done | bytes 5767184 | tf_op jit(solution)/shard_map/all_gather | solution.py:185
  149.2 8.4 %convolution_convert_fusion = bf16[768,1408]{1,0:T(8,128)(2,1)S(1)} fusion(bf16[768,2048]{1,0:T(8,128)(2,1)} %bitcast.226, bf16[2048,1408]{1,0:T(8,128)(2,1)} %all-gather.3.cloned.1.call-done), kind=kOutput, calls=%fused_computation.1 | convolution fusion | flops 4430266368 | bytes 11075584 | tf_op jit(solution)/shard_map/dot_general | solution.py:213
  157.5 1.3 copy-done.3
  158.9 1.3 collective-permute-start.13
  160.2 1.5 collective-permute-start.14
  161.9 4.2 %collective-permute-done.14 = bf16[2,1,1408]{2,1,0:T(2,128)(2,1)S(1)} collective-permute-done((bf16[2,1,1408]{2,1,0:T(2,128)(2,1)S(1)}, bf16[2,1,1408]{2,1,0:T(2,128)(2,1)S(1)}, u32[]{:S(2)}, u32[]{:S(2)}) %collective-permute-start.14) | collective-permute-done | bytes 5664 | tf_op jit(solution)/shard_map/ppermute | solution.py:24
  166.2 4.9 %multiply_add_fusion = f32[2,384,1408]{2,1,0:T(8,128)S(1)} fusion(bf16[2,384,1408]{2,1,0:T(8,128)(2,1)} %bitcast.228, bf16[2,1,1408]{2,1,0:T(2,128)(2,1)S(1)} %collective-permute-done.14, bf16[2,1,1408]{2,1,0:T(2,128)(2,1)S(1)} %collective-permute-done.13, f32[1408]{0:T(1024)S(1)} %get-tuple-element.11, f32[1408]{0:T(1024)S(1)} %get-tuple-element.10, ...), kind=kLoop, calls=%fused_computation | loop fusion | flops 15138816 | bytes 6516224 | tf_op jit(solution)/shard_map/add | solution.py:154
  171.9 36.3 %all-gather.5.cloned.1.call-done = bf16[704,2048]{1,0:T(8,128)(2,1)} async-done(((bf16[704,512]{1,0:T(8,128)(2,1)}), bf16[704,2048]{1,0:T(8,128)(2,1)}) %all-gather.5.cloned.1.call-update) | async-done | bytes 2883600 | tf_op jit(solution)/shard_map/all_gather | solution.py:186
  208.2 3.2 %convolution_convert_fusion.2 = bf16[2,2,96,1024]{3,2,0,1:T(8,128)(2,1)} fusion(bf16[704,2048]{1,0:T(8,128)(2,1)} %all-gather.5.cloned.1.call-done, bf16[2,2,96,704]{3,2,1,0:T(8,128)(2,1)S(1)} %get-tuple-element.33), kind=kOutput, calls=%fused_computation.22 | convolution fusion | flops 554041344 | bytes 2768896 | tf_op jit(solution)/shard_map/dot_general | solution.py:227
  211.4 1.7 convolution_convert_fusion.1
  213.9 2.3 convert_add_fusion.1
  216.3 1.5 collective-permute-start.16
  217.8 1.9 convert_add_fusion
  219.8 1.6 collective-permute-start.19
  221.4 6.1 %collective-permute-done.16 = bf16[2,96,1024]{2,1,0:T(8,128)(2,1)S(1)} collective-permute-done((bf16[2,96,1024]{2,1,0:T(8,128)(2,1)S(1)}, bf16[2,96,1024]{2,1,0:T(8,128)(2,1)S(1)}, u32[]{:S(2)}, u32[]{:S(2)}) %collective-permute-start.16) | collective-permute-done | bytes 393248 | tf_op jit(solution)/shard_map/ppermute | solution.py:18
  227.7 1.6 collective-permute-start.17
  229.2 2.7 %collective-permute-done.19 = bf16[2,96,1024]{2,1,0:T(8,128)(2,1)S(1)} collective-permute-done((bf16[2,96,1024]{2,1,0:T(8,128)(2,1)S(1)}, bf16[2,96,1024]{2,1,0:T(8,128)(2,1)S(1)}, u32[]{:S(2)}, u32[]{:S(2)}) %collective-permute-start.19) | collective-permute-done | bytes 393248 | tf_op jit(solution)/shard_map/ppermute | solution.py:18
  232.1 2.9 %collective-permute-done.17 = bf16[96,1024]{1,0:T(8,128)(2,1)S(1)} collective-permute-done((bf16[96,1024]{1,0:T(8,128)(2,1)S(1)}, bf16[96,1024]{1,0:T(8,128)(2,1)S(1)}, u32[]{:S(2)}, u32[]{:S(2)}) %collective-permute-start.17) | collective-permute-done | bytes 196640 | tf_op jit(solution)/shard_map/ppermute | solution.py:18
  235.0 2.7 %collective-permute-done.20 = bf16[96,1024]{1,0:T(8,128)(2,1)S(1)} collective-permute-done((bf16[96,1024]{1,0:T(8,128)(2,1)S(1)}, bf16[96,1024]{1,0:T(8,128)(2,1)S(1)}, u32[]{:S(2)}, u32[]{:S(2)}) %collective-permute-start.20) | collective-permute-done | bytes 196640 | tf_op jit(solution)/shard_map/ppermute | solution.py:18
  (134 shorter events, 27.1 us)
Async XLA Ops:
  6.5 120.9 %copy-start = (bf16[1408,512]{1,0:T(8,128)(2,1)S(1)}, bf16[1408,512]{1,0:T(8,128)(2,1)}, u32[]{:S(2)}) copy-start(bf16[1408,512]{1,0:T(8,128)(2,1)} %param.29) | copy-start | bytes 4325380
  6.5 25.0 %copy-start.7 = (bf16[512,1408]{1,0:T(8,128)(2,1)S(1)}, bf16[512,1408]{1,0:T(8,128)(2,1)}, u32[]{:S(2)}) copy-start(bf16[512,1408]{1,0:T(8,128)(2,1)} %param.26) | copy-start | bytes 4325380
  6.5 142.6 %all-gather.3.cloned.1.call-start = ((), (), s32[]{:S(2)}) async-start(), calls=%async_computation | async-start | bytes 7208960 | tf_op jit(solution)/shard_map/all_gather | solution.py:185
  6.5 82.0 %collective-permute-start.5 = (bf16[256,2048]{1,0:T(8,128)(2,1)}, bf16[256,2048]{1,0:T(8,128)(2,1)}, u32[]{:S(2)}, u32[]{:S(2)}) collective-permute-start(bf16[256,2048]{1,0:T(8,128)(2,1)} %param.23), channel_id=1, source_target_pairs={{0,1},{1,0},{2,3},{3,2},{4,5},{5,4},{6,7},{7,6},{8,9},{9,8},{10,11... | collective-permute-start | bytes 3145736 | tf_op jit(solution)/shard_map/ppermute | solution.py:18
  7.0 77.4 %collective-permute-start.7 = (bf16[256,2048]{1,0:T(8,128)(2,1)}, bf16[256,2048]{1,0:T(8,128)(2,1)}, u32[]{:S(2)}, u32[]{:S(2)}) collective-permute-start(bf16[256,2048]{1,0:T(8,128)(2,1)} %param.23), channel_id=1, source_target_pairs={{0,2},{1,3},{2,0},{3,1},{4,6},{5,7},{6,4},{7,5},{8,10},{9,11},{10,... | collective-permute-start | bytes 3145736 | tf_op jit(solution)/shard_map/ppermute | solution.py:18
  23.4 11.8 %collective-permute-start = (f32[1,136,256]{2,1,0:T(8,128)S(1)}, f32[1,136,256]{2,1,0:T(8,128)}, u32[]{:S(2)}, u32[]{:S(2)}) collective-permute-start(f32[1,136,256]{2,1,0:T(8,128)S(1)} %pad_maximum_fusion.6), channel_id=1, source_target_pairs={{0,4},{4,8},{8,12},{1,5},{5,9},{9,13},{2,6},{6,10},{10,14},{3,7},{... | collective-permute-start | bytes 417800 | tf_op jit(solution)/shard_map/ppermute | solution.py:24
  30.2 8.7 %collective-permute-start.2 = (f32[1,136,256]{2,1,0:T(8,128)S(1)}, f32[1,136,256]{2,1,0:T(8,128)}, u32[]{:S(2)}, u32[]{:S(2)}) collective-permute-start(f32[1,136,256]{2,1,0:T(8,128)S(1)} %pad_maximum_fusion.8), channel_id=1, source_target_pairs={{4,0},{8,4},{12,8},{5,1},{9,5},{13,9},{6,2},{10,6},{14,10},{7,3},{... | collective-permute-start | bytes 417800 | tf_op jit(solution)/shard_map/ppermute | solution.py:24
  35.1 20.4 %copy-start.10 = (bf16[384,256]{1,0:T(8,128)(2,1)S(1)}, bf16[384,256]{1,0:T(8,128)(2,1)}, u32[]{:S(2)}) copy-start(bf16[384,256]{1,0:T(8,128)(2,1)} %param.19) | copy-start | bytes 589828
  35.1 43.3 %copy-start.9 = (bf16[384,128]{1,0:T(8,128)(2,1)S(1)}, bf16[384,128]{1,0:T(8,128)(2,1)}, u32[]{:S(2)}) copy-start(bf16[384,128]{1,0:T(8,128)(2,1)} %param.16) | copy-start | bytes 294916
  35.1 45.2 %copy-start.5 = (bf16[384,128]{1,0:T(8,128)(2,1)S(1)}, bf16[384,128]{1,0:T(8,128)(2,1)}, u32[]{:S(2)}) copy-start(bf16[384,128]{1,0:T(8,128)(2,1)} %param.17) | copy-start | bytes 294916
  35.1 173.1 %all-gather.5.cloned.1.call-start = ((), (), s32[]{:S(2)}) async-start(), calls=%async_computation.1 | async-start | bytes 3604480 | tf_op jit(solution)/shard_map/all_gather | solution.py:186
  45.7 35.0 %copy-start.6 = (bf16[384,256]{1,0:T(8,128)(2,1)S(1)}, bf16[384,256]{1,0:T(8,128)(2,1)}, u32[]{:S(2)}) copy-start(bf16[384,256]{1,0:T(8,128)(2,1)} %param.18) | copy-start | bytes 589828
  45.7 30.6 %collective-permute-start.1 = (f32[1,136,256]{2,1,0:T(8,128)S(1)}, f32[1,136,256]{2,1,0:T(8,128)S(1)}, u32[]{:S(2)}, u32[]{:S(2)}) collective-permute-start(f32[1,136,256]{2,1,0:T(8,128)S(1)} %pad_maximum_fusion.7), channel_id=1, source_target_pairs={{0,8},{4,12},{1,9},{5,13},{2,10},{6,14},{3,11},{7,15},{16,24},{20,... | collective-permute-start | bytes 417800 | tf_op jit(solution)/shard_map/ppermute | solution.py:24
  53.8 20.8 %collective-permute-start.3 = (f32[1,136,256]{2,1,0:T(8,128)S(1)}, f32[1,136,256]{2,1,0:T(8,128)S(1)}, u32[]{:S(2)}, u32[]{:S(2)}) collective-permute-start(f32[1,136,256]{2,1,0:T(8,128)S(1)} %pad_maximum_fusion.9), channel_id=1, source_target_pairs={{8,0},{12,4},{9,1},{13,5},{10,2},{14,6},{11,3},{15,7},{24,16},{28,... | collective-permute-start | bytes 417800 | tf_op jit(solution)/shard_map/ppermute | solution.py:24
  82.6 2.1 copy-start.14
  84.5 8.2 %collective-permute-start.9 = (bf16[256,2048]{1,0:T(8,128)(2,1)}, bf16[256,2048]{1,0:T(8,128)(2,1)S(1)}, u32[]{:S(2)}, u32[]{:S(2)}) collective-permute-start(bf16[256,2048]{1,0:T(8,128)(2,1)} %collective-permute-done.7), channel_id=1, source_target_pairs={{0,1},{1,0},{2,3},{3,2},{4,5},{5,4},{6,7},{7,6},{8,9},{9,8},{10,11... | collective-permute-start | bytes 3145736 | tf_op jit(solution)/shard_map/ppermute | solution.py:18
  85.0 3.5 %collective-permute-start.4 = (bf16[96,256]{1,0:T(8,128)(2,1)S(1)}, bf16[96,256]{1,0:T(8,128)(2,1)S(1)}, u32[]{:S(2)}, u32[]{:S(2)}) collective-permute-start(bf16[96,256]{1,0:T(8,128)(2,1)S(1)} %get-tuple-element.36), channel_id=1, source_target_pairs={{0,1},{1,0},{2,3},{3,2},{4,5},{5,4},{6,7},{7,6},{8,9},{9,8},{10,11... | collective-permute-start | bytes 147464 | tf_op jit(solution)/shard_map/ppermute | solution.py:18
  87.0 4.2 %collective-permute-start.6 = (bf16[96,256]{1,0:T(8,128)(2,1)S(1)}, bf16[96,256]{1,0:T(8,128)(2,1)S(1)}, u32[]{:S(2)}, u32[]{:S(2)}) collective-permute-start(bf16[96,256]{1,0:T(8,128)(2,1)S(1)} %get-tuple-element.35), channel_id=1, source_target_pairs={{0,2},{1,3},{2,0},{3,1},{4,6},{5,7},{6,4},{7,5},{8,10},{9,11},{10,... | collective-permute-start | bytes 147464 | tf_op jit(solution)/shard_map/ppermute | solution.py:18
  88.3 4.4 %copy-start.8 = (bf16[96,2048]{1,0:T(8,128)(2,1)S(1)}, bf16[96,2048]{1,0:T(8,128)(2,1)}, u32[]{:S(2)}) copy-start(bf16[96,2048]{1,0:T(8,128)(2,1)} %param.15) | copy-start | bytes 1179652
  88.3 4.3 %collective-permute-start.8 = (bf16[96,256]{1,0:T(8,128)(2,1)S(1)}, bf16[96,256]{1,0:T(8,128)(2,1)S(1)}, u32[]{:S(2)}, u32[]{:S(2)}) collective-permute-start(bf16[96,256]{1,0:T(8,128)(2,1)S(1)} %get-tuple-element.34), channel_id=1, source_target_pairs={{0,3},{1,2},{2,1},{3,0},{4,7},{5,6},{6,5},{7,4},{8,11},{9,10},{10,... | collective-permute-start | bytes 147464 | tf_op jit(solution)/shard_map/ppermute | solution.py:18
  92.7 0.7 copy-start.11
  93.5 10.7 %collective-permute-start.10 = (bf16[96,2048]{1,0:T(8,128)(2,1)S(1)}, bf16[96,2048]{1,0:T(8,128)(2,1)S(1)}, u32[]{:S(2)}, u32[]{:S(2)}) collective-permute-start(bf16[96,2048]{1,0:T(8,128)(2,1)S(1)} %multiply_convert_fusion), channel_id=1, source_target_pairs={{0,16},{16,0},{1,17},{17,1},{2,18},{18,2},{3,19},{19,3},{4,20},{20... | collective-permute-start | bytes 1179656 | tf_op jit(solution)/shard_map/ppermute | solution.py:18
  104.2 2.3 copy-start.4
  105.2 18.6 %collective-permute-start.11 = (bf16[2,96,2048]{2,1,0:T(8,128)(2,1)}, bf16[2,96,2048]{2,1,0:T(8,128)(2,1)}, u32[]{:S(2)}, u32[]{:S(2)}) collective-permute-start(bf16[2,96,2048]{2,1,0:T(8,128)(2,1)} %pad_maximum_fusion.5), channel_id=1, source_target_pairs={{0,2},{1,3},{2,0},{3,1},{4,6},{5,7},{6,4},{7,5},{8,10},{9,11},{10,... | collective-permute-start | bytes 2359304 | tf_op jit(solution)/shard_map/ppermute | solution.py:18
  125.2 0.9 copy-start.2
  127.4 3.8 %collective-permute-start.12 = (bf16[2,2,96,2048]{3,2,0,1:T(8,128)(2,1)}, bf16[2,2,96,2048]{3,2,0,1:T(8,128)(2,1)}, u32[]{:S(2)}, u32[]{:S(2)}) collective-permute-start(bf16[2,2,96,2048]{3,2,0,1:T(8,128)(2,1)} %pad_maximum_fusion.3), channel_id=1, source_target_pairs={{0,1},{1,0},{2,3},{3,2},{4,5},{5,4},{6,7},{7,6},{8,9},{9,8},{10,11... | collective-permute-start | bytes 4718600 | tf_op jit(solution)/shard_map/ppermute | solution.py:18
  149.2 12.6 %copy-start.12 = (f32[3,1408]{1,0:T(4,128)S(1)}, f32[3,1408]{1,0:T(4,128)}, u32[]{:S(2)}) copy-start(f32[3,1408]{1,0:T(4,128)} %param.28) | copy-start | bytes 50692
  149.2 12.6 %copy-start.13 = (f32[3,1408]{1,0:T(4,128)S(1)}, f32[3,1408]{1,0:T(4,128)}, u32[]{:S(2)}) copy-start(f32[3,1408]{1,0:T(4,128)} %param.27) | copy-start | bytes 50692
  157.5 1.4 copy-start.3
  158.9 3.0 %collective-permute-start.13 = (bf16[2,1,1408]{2,1,0:T(2,128)(2,1)S(1)}, bf16[2,1,1408]{2,1,0:T(2,128)(2,1)S(1)}, u32[]{:S(2)}, u32[]{:S(2)}) collective-permute-start(bf16[2,1,1408]{2,1,0:T(2,128)(2,1)S(1)} %get-tuple-element.28), channel_id=1, source_target_pairs={{0,4},{4,8},{8,12},{1,5},{5,9},{9,13},{2,6},{6,10},{10,14},{3,7},{... | collective-permute-start | bytes 16904 | tf_op jit(solution)/shard_map/ppermute | solution.py:24
  160.2 6.0 %collective-permute-start.14 = (bf16[2,1,1408]{2,1,0:T(2,128)(2,1)S(1)}, bf16[2,1,1408]{2,1,0:T(2,128)(2,1)S(1)}, u32[]{:S(2)}, u32[]{:S(2)}) collective-permute-start(bf16[2,1,1408]{2,1,0:T(2,128)(2,1)S(1)} %get-tuple-element.29), channel_id=1, source_target_pairs={{4,0},{8,4},{12,8},{5,1},{9,5},{13,9},{6,2},{10,6},{14,10},{7,3},{... | collective-permute-start | bytes 16904 | tf_op jit(solution)/shard_map/ppermute | solution.py:24
  208.2 3.2 %copy-start.15 = (bf16[704,2048]{1,0:T(8,128)(2,1)S(1)}, bf16[704,2048]{1,0:T(8,128)(2,1)}, u32[]{:S(2)}) copy-start(bf16[704,2048]{1,0:T(8,128)(2,1)} %all-gather.5.cloned.1.call-done) | copy-start | bytes 8650756
  211.4 2.5 %collective-permute-start.15 = (bf16[2,2,96,1024]{3,2,0,1:T(8,128)(2,1)}, bf16[2,2,96,1024]{3,2,0,1:T(8,128)(2,1)S(1)}, u32[]{:S(2)}, u32[]{:S(2)}) collective-permute-start(bf16[2,2,96,1024]{3,2,0,1:T(8,128)(2,1)} %convolution_convert_fusion.2), channel_id=1, source_target_pairs={{0,1},{1,0},{2,3},{3,2},{4,5},{5,4},{6,7},{7,6},{8,9},{9,8},{10,11... | collective-permute-start | bytes 2359304 | tf_op jit(solution)/shard_map/ppermute | solution.py:18
  213.1 4.7 %collective-permute-start.18 = (bf16[2,2,96,1024]{3,2,1,0:T(8,128)(2,1)}, bf16[2,2,96,1024]{3,2,1,0:T(8,128)(2,1)}, u32[]{:S(2)}, u32[]{:S(2)}) collective-permute-start(bf16[2,2,96,1024]{3,2,1,0:T(8,128)(2,1)} %convolution_convert_fusion.1), channel_id=1, source_target_pairs={{0,1},{1,0},{2,3},{3,2},{4,5},{5,4},{6,7},{7,6},{8,9},{9,8},{10,11... | collective-permute-start | bytes 2359304 | tf_op jit(solution)/shard_map/ppermute | solution.py:18
  213.9 3.9 %copy-start.16 = (bf16[704,2048]{1,0:T(8,128)(2,1)S(1)}, bf16[704,2048]{1,0:T(8,128)(2,1)}, u32[]{:S(2)}) copy-start(bf16[704,2048]{1,0:T(8,128)(2,1)} %all-gather.5.cloned.1.call-done) | copy-start | bytes 8650756
  216.3 11.2 %collective-permute-start.16 = (bf16[2,96,1024]{2,1,0:T(8,128)(2,1)S(1)}, bf16[2,96,1024]{2,1,0:T(8,128)(2,1)S(1)}, u32[]{:S(2)}, u32[]{:S(2)}) collective-permute-start(bf16[2,96,1024]{2,1,0:T(8,128)(2,1)S(1)} %fusion.19), channel_id=1, source_target_pairs={{0,2},{1,3},{2,0},{3,1},{4,6},{5,7},{6,4},{7,5},{8,10},{9,11},{10,... | collective-permute-start | bytes 1179656 | tf_op jit(solution)/shard_map/ppermute | solution.py:18
  219.8 12.1 %collective-permute-start.19 = (bf16[2,96,1024]{2,1,0:T(8,128)(2,1)S(1)}, bf16[2,96,1024]{2,1,0:T(8,128)(2,1)S(1)}, u32[]{:S(2)}, u32[]{:S(2)}) collective-permute-start(bf16[2,96,1024]{2,1,0:T(8,128)(2,1)S(1)} %fusion.20), channel_id=1, source_target_pairs={{0,16},{16,0},{1,17},{17,1},{2,18},{18,2},{3,19},{19,3},{4,20},{20... | collective-permute-start | bytes 1179656 | tf_op jit(solution)/shard_map/ppermute | solution.py:18
  227.7 7.3 %collective-permute-start.17 = (bf16[96,1024]{1,0:T(8,128)(2,1)S(1)}, bf16[96,1024]{1,0:T(8,128)(2,1)S(1)}, u32[]{:S(2)}, u32[]{:S(2)}) collective-permute-start(bf16[96,1024]{1,0:T(8,128)(2,1)S(1)} %fusion.45), channel_id=1, source_target_pairs={{0,16},{16,0},{1,17},{17,1},{2,18},{18,2},{3,19},{19,3},{4,20},{20... | collective-permute-start | bytes 589832 | tf_op jit(solution)/shard_map/ppermute | solution.py:18
  231.9 6.8 %copy-start.1 = (bf16[1408,512]{1,0:T(8,128)(2,1)S(1)}, bf16[1408,512]{1,0:T(8,128)(2,1)}, u32[]{:S(2)}) copy-start(bf16[1408,512]{1,0:T(8,128)(2,1)} %param.29) | copy-start | bytes 4325380
  232.0 5.7 %collective-permute-start.20 = (bf16[96,1024]{1,0:T(8,128)(2,1)S(1)}, bf16[96,1024]{1,0:T(8,128)(2,1)S(1)}, u32[]{:S(2)}, u32[]{:S(2)}) collective-permute-start(bf16[96,1024]{1,0:T(8,128)(2,1)S(1)} %fusion.44), channel_id=1, source_target_pairs={{0,2},{1,3},{2,0},{3,1},{4,6},{5,7},{6,4},{7,5},{8,10},{9,11},{10,... | collective-permute-start | bytes 589832 | tf_op jit(solution)/shard_map/ppermute | solution.py:18
Sparse Core Ops, SparseCore 0:
  35.2 113.8 all-gather.2
  150.7 57.4 all-gather.4
